TPU v7x, 32 devices: a whole 2x2x4 slice. The times are simulated.
32 devices in a mesh: grp: 2 (over y), sp: 4 (over z), tp: 4 (over x, core).
Axes of the slice: x: 2, y: 2, z: 4, core: 2. Of those that a mesh axis runs over, the one named last changes fastest.
Arguments:
- recept: bfloat16 [4096, 2048], P(('grp', 'sp'), 'tp'), parts along dimension 0, may hold values from -6 to 6
- key_input: bfloat16 [4096, 2048], P(('grp', 'sp'), 'tp'), parts along dimension 0, may hold values from -6 to 6
- value_input: bfloat16 [4096, 2048], P(('grp', 'sp'), 'tp'), parts along dimension 0, may hold values from -6 to 6
- output_gate_input: bfloat16 [4096, 2048], P(('grp', 'sp'), 'tp'), parts along dimension 0, may hold values from -6 to 6
- decay_input_part: bfloat16 [4096, 2048], P(('grp', 'sp'), 'tp'), parts along dimension 0, may hold values from -4.8 to 4.8
- correction_rate_input: bfloat16 [4096, 2048], P(('grp', 'sp'), 'tp'), parts along dimension 0, may hold values from -4 to 4
- head_decay_offset: float32 [4096, 32], P(('grp', 'sp'), 'tp'), parts along dimension 0, may hold values from -2.1 to 0
- decay_fixed_bias: float32 [2048], P('tp'), may hold values from -11.5 to -2.8
- correction_rate_bias: float32 [2048], P('tp'), may hold values from -8.5 to 1
- head_norm_gain: float32 [2048], P('tp'), may hold values from 0.1 to 1.9
- self_term_weight: float32 [2048], P('tp'), may hold values from -2 to 2
- output_weight_matrix: bfloat16 [2048, 2048], P('tp'), may hold values from -0.125 to 0.125
- residual: bfloat16 [4096, 2048], P(('grp', 'sp', 'tp')), parts along dimension 0, may hold values from -6 to 6
- feedforward_norm_gain: float32 [2048], replicated, may hold values from 0.1 to 1.9
- routed_expert_index: int32 [4096, 2], P(('grp', 'sp', 'tp')), parts along dimension 0, may hold values from 0 to 3, all different within a row; in each aligned block of 128 rows (0 to 127, 128 to 255, ...) at most 96 rows name the same one
- routed_expert_weight: float32 [4096, 2], P(('grp', 'sp', 'tp')), parts along dimension 0, may hold values from 0.2 to 1
- gate_weight_experts: bfloat16 [4, 2048, 1024], P('sp', None, 'tp'), may hold values from -0.125 to 0.125
- up_weight_experts: bfloat16 [4, 2048, 1024], P('sp', None, 'tp'), may hold values from -0.125 to 0.125
- down_weight_experts: bfloat16 [4, 1024, 2048], P('sp', 'tp'), may hold values from -0.1875 to 0.1875
Outputs:
- output: bfloat16 [4096, 2048], P(('grp', 'sp', 'tp')), parts along dimension 0
There are 2 independent parts, one for each index of `grp`. A program takes and returns all parts, laid end to end along the dimension named above; an argument that names none is the same for every part. Nothing has to cross between parts.
Inputs may be any that keep to these rules, and one draw needn't show every extreme that they name: `routed_expert_index`: in each aligned block of 128 rows (the rows of one device) no expert is named by more than 96 routes; the two experts of a row differ.
All inputs are finite; a program needn't handle non-finite values.
Results may differ from a plain program's by a relative error of at most 0.0058.
Values may be sent and summed in bfloat16 or wider, within the bound.
A program may use at most 128 MiB of HBM per device.

v0:
```python
import functools

import jax
import jax.numpy as jnp
from jax import lax
from jax.experimental import pallas as pl
from jax.experimental.pallas import tpu as pltpu
from jax.sharding import PartitionSpec as P

SPAN = 64
SUB = 16
LANES = 256
GROUP_EPS = 0.00064
NORM_EPS = 1e-06
NN = (((1,), (0,)), ((), ()))
NT = (((1,), (1,)), ((), ()))
TN = (((0,), (0,)), ((), ()))


def halves(x):
    high = x.astype(jnp.bfloat16)
    return high, (x - high.astype(jnp.float32)).astype(jnp.bfloat16)


def product(left, right, dims):
    def dot(a, b):
        return lax.dot_general(a, b, dims, preferred_element_type=jnp.float32)

    return dot(left[0], right[0]) + (dot(left[1], right[0]) + dot(left[0], right[1]))


def block_mask(head_width):
    rows = lax.broadcasted_iota(jnp.int32, (LANES, LANES), 0) // head_width
    lanes = lax.broadcasted_iota(jnp.int32, (LANES, LANES), 1) // head_width
    return jnp.where(rows == lanes, 1.0, 0.0)


def spread_blocks(x, mask):
    copies = LANES // x.shape[0]
    return tuple(jnp.concatenate([part] * copies, axis=0) * mask for part in halves(x))


def head_sum(x, mask):
    high, low = halves(x)
    return lax.dot_general(
        high, mask, NN, preferred_element_type=jnp.float32
    ) + lax.dot_general(low, mask, NN, preferred_element_type=jnp.float32)


def chunk_kernel(
    head_width,
    recept_ref,
    key_ref,
    value_ref,
    decay_ref,
    rate_ref,
    offset_ref,
    decay_bias_ref,
    rate_bias_ref,
    map_ref,
    own_ref,
    transit_ref,
    added_ref,
):
    span = head_width
    wide_mask = block_mask(head_width)
    mask = wide_mask.astype(jnp.bfloat16)
    per_group = LANES // head_width
    times = lax.broadcasted_iota(jnp.int32, (span, LANES), 0)
    lanes = lax.broadcasted_iota(jnp.int32, (span, LANES), 1)
    earlier = lanes % head_width
    strict = times > earlier
    within = times >= earlier
    eye = jnp.where(times == earlier, 1.0, 0.0)
    same = (times // SUB) == (earlier // SUB)
    tri = jnp.where(
        lax.broadcasted_iota(jnp.int32, (span, span), 0)
        >= lax.broadcasted_iota(jnp.int32, (span, span), 1),
        1.0,
        0.0,
    ).astype(jnp.bfloat16)

    @pl.when(pl.program_id(0) == 0)
    def _():
        full_lanes = lax.broadcasted_iota(jnp.int32, transit_ref.shape, 1) % head_width
        full_rows = lax.broadcasted_iota(jnp.int32, transit_ref.shape, 0)
        transit_ref[...] = jnp.where(full_lanes == full_rows, 1.0, 0.0)
        added_ref[...] = jnp.zeros_like(added_ref)

    spread = functools.partial(spread_blocks, mask=mask)
    row_count, channel_width = recept_ref.shape
    cells = [
        (group, chunk)
        for chunk in range(row_count // span)
        for group in range(channel_width // LANES)
    ]

    def prepare(group, chunk):
        at = (slice(chunk * span, (chunk + 1) * span), slice(group * LANES, (group + 1) * LANES))
        cols = at[1]
        recept = recept_ref[at].astype(jnp.float32)
        key = key_ref[at].astype(jnp.float32)
        value = value_ref[at].astype(jnp.float32)
        offset = jnp.zeros((span, LANES), jnp.float32)
        for head in range(per_group):
            column = group * per_group + head
            offset = jnp.where(
                lanes // head_width == head, offset_ref[at[0], column : column + 1], offset
            )
        pre = decay_bias_ref[:, cols] + decay_ref[at].astype(jnp.float32)
        decay = offset - 0.6065306597126334 / (1.0 + jnp.exp(-pre))
        rate = 1.0 / (
            1.0 + jnp.exp(-(rate_bias_ref[:, cols] + rate_ref[at].astype(jnp.float32)))
        )
        unit = key * lax.rsqrt(head_sum(key * key, mask) + NORM_EPS)
        one, rest = halves(decay)
        third = (decay - one.astype(jnp.float32) - rest.astype(jnp.float32)).astype(jnp.bfloat16)
        cumul = sum(
            lax.dot_general(tri, part, NN, preferred_element_type=jnp.float32)
            for part in (third, rest, one)
        )
        middle = cumul[span // 2 : span // 2 + 1]
        last = cumul[span - 1 : span]
        center = cumul - middle
        shrink = jnp.exp(center)
        grow = jnp.exp(-center)
        remove = -unit * jnp.exp(center - decay)
        reads = recept * shrink
        write = unit * rate * grow
        keys = key * grow
        left = halves(jnp.concatenate([remove, reads], axis=0))
        by_write = product(left, spread(write), NT)
        by_key = product(left, spread(keys), NT)
        remove_write = jnp.where(strict, by_write[:span], 0.0)
        read_write = halves(jnp.where(within, by_write[span:], 0.0))
        key_rows = halves(
            jnp.concatenate(
                [jnp.where(strict, by_key[:span], 0.0), jnp.where(within, by_key[span:], 0.0)],
                axis=0,
            )
        )
        power = jnp.where(same, remove_write, 0.0)
        inverse = eye + power
        power = product(halves(power), spread(power), NN)
        reach = 2
        while reach < SUB:
            factor = spread(power)
            if reach * 2 < SUB:
                both = product(
                    halves(jnp.concatenate([inverse, power], axis=0)), factor, NN
                )
                inverse = inverse + both[:span]
                power = both[span:]
            else:
                inverse = inverse + product(halves(inverse), factor, NN)
            reach *= 2
        size = SUB
        while size < span:
            joint = (times // (2 * size) == earlier // (2 * size)) & (
                times // size != earlier // size
            )
            step = product(
                halves(inverse), spread(jnp.where(joint, remove_write, 0.0)), NN
            )
            inverse = inverse + product(halves(step), spread(inverse), NN)
            size *= 2
        inverse = halves(inverse)
        start = jnp.exp(middle)
        from_value = product(key_rows, spread(value), NN)
        inv_remove = product(inverse, spread(remove), NN) * start
        inv_value = product(inverse, spread(from_value[:span]), NN)
        read_map = reads * start + product(read_write, spread(inv_remove), NN)
        read_own = from_value[span:] + product(read_write, spread(inv_value), NN)
        tail = jnp.exp(last - middle)
        write_end = write * tail
        key_end = keys * tail
        transit = product(halves(inv_remove.T), halves(write_end), NN)
        transit = transit * wide_mask
        full = jnp.concatenate([jnp.exp(last)] * (LANES // 8), axis=0)
        full = jnp.concatenate([full] * 8, axis=0)
        diagonal = lax.broadcasted_iota(jnp.int32, (LANES, LANES), 0) == (
            lax.broadcasted_iota(jnp.int32, (LANES, LANES), 1)
        )
        transit = transit + jnp.where(diagonal, full, 0.0)
        added = product(
            halves(jnp.concatenate([inv_value, value], axis=0).T),
            halves(jnp.concatenate([write_end, key_end], axis=0)),
            NN,
        )
        added = added * wide_mask
        added = sum(added[h * head_width : (h + 1) * head_width] for h in range(per_group))
        return at, read_map, read_own, transit, added

    for group, chunk in cells:
        at, read_map, read_own, transit, added = prepare(group, chunk)
        cols = at[1]
        held_transit = transit_ref[:, cols]
        held_added = added_ref[:, cols]
        rows = halves(read_map)
        map_ref[at] = product(rows, spread(held_transit), NT)
        own_ref[at] = read_own + product(rows, spread(held_added), NT)
        moved = product(
            halves(jnp.concatenate([held_transit, held_added], axis=0)), halves(transit), NN
        )
        transit_ref[:, cols] = moved[:span]
        added_ref[:, cols] = moved[span:] + added


def advance_kernel(head_width, state_ref, transit_ref, added_ref, out_ref):
    mask = block_mask(head_width).astype(jnp.bfloat16)
    for group in range(state_ref.shape[1] // LANES):
        cols = slice(group * LANES, (group + 1) * LANES)
        out_ref[:, cols] = added_ref[:, cols] + product(
            halves(state_ref[:, cols]), spread_blocks(transit_ref[:, cols], mask), NN
        )


def finish_kernel(
    head_width,
    map_ref,
    own_ref,
    state_ref,
    recept_ref,
    key_ref,
    value_ref,
    gate_ref,
    gain_ref,
    self_ref,
    out_ref,
):
    mask = block_mask(head_width).astype(jnp.bfloat16)
    for group in range(map_ref.shape[1] // LANES):
        cols = slice(group * LANES, (group + 1) * LANES)
        read = own_ref[:, cols] + product(
            halves(map_ref[:, cols]), spread_blocks(state_ref[:, cols], mask), NT
        )
        off = read - head_sum(read, mask) * (1.0 / head_width)
        spread = head_sum(off * off, mask) * (1.0 / head_width)
        normed = off * lax.rsqrt(spread + GROUP_EPS) * gain_ref[:, cols]
        own = head_sum(
            recept_ref[:, cols].astype(jnp.float32)
            * key_ref[:, cols].astype(jnp.float32)
            * self_ref[:, cols],
            mask,
        ) * value_ref[:, cols].astype(jnp.float32)
        out_ref[:, cols] = ((normed + own) * gate_ref[:, cols].astype(jnp.float32)).astype(
            jnp.bfloat16
        )


def mixer(
    recept,
    key_input,
    value_input,
    output_gate_input,
    decay_input_part,
    correction_rate_input,
    head_decay_offset,
    decay_fixed_bias,
    correction_rate_bias,
    head_norm_gain,
    self_term_weight,
    axis_size,
):
    length, width = recept.shape
    heads = head_decay_offset.shape[1]
    head_width = width // heads
    rows = 2 * SPAN
    by_rows = pl.BlockSpec((rows, width), lambda i: (i, 0))
    fixed = pl.BlockSpec((1, width), lambda i: (0, 0))
    states = pl.BlockSpec((head_width, width), lambda i: (0, 0))
    wide = jax.ShapeDtypeStruct((length, width), jnp.float32)
    small = jax.ShapeDtypeStruct((head_width, width), jnp.float32)
    params = pltpu.CompilerParams(dimension_semantics=("arbitrary",))
    read_map, read_own, transit, added = pl.pallas_call(
        functools.partial(chunk_kernel, head_width),
        grid=(length // rows,),
        in_specs=[by_rows] * 5
        + [pl.BlockSpec((rows, heads), lambda i: (i, 0)), fixed, fixed],
        out_specs=[by_rows, by_rows, states, states],
        out_shape=[wide, wide, small, small],
        compiler_params=params,
        cost_estimate=pl.CostEstimate(
            flops=30_000_000_000, bytes_accessed=8 * length * width, transcendentals=0
        ),
        name="chunks",
    )(
        recept,
        key_input,
        value_input,
        decay_input_part,
        correction_rate_input,
        head_decay_offset,
        decay_fixed_bias[None],
        correction_rate_bias[None],
    )
    place = lax.axis_index("sp")
    state = jnp.zeros_like(added)
    for lap in range(axis_size - 1):
        sent = added
        if lap > 0:
            sent = pl.pallas_call(
                functools.partial(advance_kernel, head_width), out_shape=small, name="advance"
            )(state, transit, added)
        got = lax.ppermute(sent, "sp", [(i, i + 1) for i in range(axis_size - 1)])
        state = jnp.where(place == lap + 1, got, state)
    return pl.pallas_call(
        functools.partial(finish_kernel, head_width),
        grid=(length // rows,),
        in_specs=[by_rows, by_rows, states] + [by_rows] * 4 + [fixed, fixed],
        out_specs=by_rows,
        out_shape=jax.ShapeDtypeStruct((length, width), jnp.bfloat16),
        compiler_params=params,
        cost_estimate=pl.CostEstimate(
            flops=4_000_000_000, bytes_accessed=20 * length * width, transcendentals=0
        ),
        name="finish",
    )(
        read_map,
        read_own,
        state,
        recept,
        key_input,
        value_input,
        output_gate_input,
        head_norm_gain[None],
        self_term_weight[None],
    )


def local(
    recept,
    key_input,
    value_input,
    output_gate_input,
    decay_input_part,
    correction_rate_input,
    head_decay_offset,
    decay_fixed_bias,
    correction_rate_bias,
    head_norm_gain,
    self_term_weight,
    output_weight_matrix,
    residual,
    feedforward_norm_gain,
    routed_expert_index,
    routed_expert_weight,
    gate_weight_experts,
    up_weight_experts,
    down_weight_experts,
):
    gates = lax.all_gather(gate_weight_experts, "tp", axis=0)
    ups = lax.all_gather(up_weight_experts, "tp", axis=0)
    downs = lax.all_gather(down_weight_experts, "tp", axis=0)
    attention_result = mixer(
        recept,
        key_input,
        value_input,
        output_gate_input,
        decay_input_part,
        correction_rate_input,
        head_decay_offset,
        decay_fixed_bias,
        correction_rate_bias,
        head_norm_gain,
        self_term_weight,
        lax.axis_size("sp"),
    )
    part = jnp.dot(
        attention_result, output_weight_matrix, preferred_element_type=jnp.float32
    ).astype(jnp.bfloat16)
    part, gates, ups, downs = lax.optimization_barrier((part, gates, ups, downs))
    proj = lax.psum_scatter(part, "tp", scatter_dimension=0, tiled=True)
    stream = residual.astype(jnp.float32) + lax.optimization_barrier(proj).astype(jnp.float32)
    ffn_in = (
        stream
        * lax.rsqrt(jnp.mean(stream * stream, axis=-1, keepdims=True) + NORM_EPS)
        * feedforward_norm_gain
    ).astype(jnp.bfloat16)
    width = ffn_in.shape[1]
    local_experts = gate_weight_experts.shape[0]
    experts = local_experts * lax.axis_size("sp")
    ids = jnp.arange(experts, dtype=jnp.int32)
    shares = jnp.sum(
        jnp.where(
            routed_expert_index[:, :, None] == ids, routed_expert_weight[:, :, None], 0.0
        ),
        axis=1,
    )
    first = shares.astype(jnp.bfloat16)
    rest = shares - first.astype(jnp.float32)
    second = rest.astype(jnp.bfloat16)
    third = (rest - second.astype(jnp.float32)).astype(jnp.bfloat16)
    extra = jnp.concatenate([first, second, third], axis=1)
    extra = jnp.pad(extra, ((0, 0), (0, -extra.shape[1] % 128)))
    packed = lax.all_gather(
        jnp.concatenate([ffn_in, extra], axis=1), "sp", axis=0, tiled=True
    )
    features = packed[:, :width]
    tail = packed[:, width : width + 3 * experts].astype(jnp.float32)
    shares = tail[:, :experts] + tail[:, experts : 2 * experts] + tail[:, 2 * experts :]
    total = None
    for own in range(local_experts):
        expert = lax.axis_index("sp") * local_experts + own
        share = jnp.sum(jnp.where(ids[None, :] == expert, shares, 0.0), axis=1, keepdims=True)
        gated = jnp.einsum(
            "rd,jdf->jrf", features, gates[:, own], preferred_element_type=jnp.float32
        )
        upward = jnp.einsum(
            "rd,jdf->jrf", features, ups[:, own], preferred_element_type=jnp.float32
        )
        hidden = (jax.nn.silu(gated) * upward).astype(jnp.bfloat16)
        result = jnp.einsum(
            "jrf,jfd->rd", hidden, downs[:, own], preferred_element_type=jnp.float32
        )
        term = result * share
        total = term if total is None else total + term
    weighted = lax.psum_scatter(
        total.astype(jnp.bfloat16), "sp", scatter_dimension=0, tiled=True
    )
    return (stream + weighted.astype(jnp.float32)).astype(jnp.bfloat16)


def solution(mesh):
    return jax.shard_map(
        local,
        mesh=mesh,
        in_specs=(
            P(("grp", "sp"), "tp"),
            P(("grp", "sp"), "tp"),
            P(("grp", "sp"), "tp"),
            P(("grp", "sp"), "tp"),
            P(("grp", "sp"), "tp"),
            P(("grp", "sp"), "tp"),
            P(("grp", "sp"), "tp"),
            P("tp"),
            P("tp"),
            P("tp"),
            P("tp"),
            P("tp", None),
            P(("grp", "sp", "tp"), None),
            P(),
            P(("grp", "sp", "tp"), None),
            P(("grp", "sp", "tp"), None),
            P("sp", None, "tp"),
            P("sp", None, "tp"),
            P("sp", "tp", None),
        ),
        out_specs=P(("grp", "sp", "tp"), None),
        check_vma=False,
    )
```

profile of v0, /device:TPU:0, one launch (start us, length us, event | category | flops | bytes accessed | tf_op | source)
XLA Modules:
  0.0 268.0 jit_solution(940754056100755142)
XLA Ops:
  6.5 0.0 copy-start
  6.5 0.0 all-gather.10.cloned.1.call-start
  6.5 0.7 all-gather.10.cloned.1.call-update
  7.3 0.0 all-gather.12.cloned.1.call-start
  7.3 0.7 all-gather.12.cloned.1.call-update
  8.0 0.0 all-gather.14.cloned.1.call-start
  8.1 0.7 all-gather.14.cloned.1.call-update
  8.7 0.0 reduce-scatter.3.cloned.1.call-start
  8.8 0.0 copy-done.3
  8.8 0.8 copy.31.offset_ref
  9.6 54.6 %chunks.1 = (f32[512,512]{1,0:T(8,128)}, f32[512,512]{1,0:T(8,128)}, f32[64,512]{1,0:T(8,128)}, f32[64,512]{1,0:T(8,128)}) custom-call(bf16[512,512]{1,0:T(8,128)(2,1)} %recept_ref.3, bf16[512,512]{1,0:T(8,128)(2,1)} %key_ref.3, bf16[512,512]{1,0:T(8,128)(2,1)} %value_ref.3, bf16[512,512]{1,0:T(8,128)(2,1)} %decay_ref.1, bf16[512,512]{1,0:T(8,128)(2,1)} %rate_ref.1, ...), custom_call_target="tpu_custom_call" | custom-call | flops 30000001024 | bytes 2097152 | tf_op jit(solution)/shard_map/chunks/pallas_call | solution.py:275
  64.2 5.0 %collective-permute-start = (f32[64,512]{1,0:T(8,128)}, f32[64,512]{1,0:T(8,128)S(1)}, u32[]{:S(2)}, u32[]{:S(2)}) collective-permute-start(f32[64,512]{1,0:T(8,128)} %get-tuple-element.15.added_ref), channel_id=1, source_target_pairs={{0,4},{4,8},{8,12},{1,5},{5,9},{9,13},{2,6},{6,10},{10,14},{3,7},{... | collective-permute-start | bytes 393224 | tf_op jit(solution)/shard_map/ppermute | solution.py:305
  69.2 3.0 %collective-permute-done = f32[64,512]{1,0:T(8,128)S(1)} collective-permute-done((f32[64,512]{1,0:T(8,128)}, f32[64,512]{1,0:T(8,128)S(1)}, u32[]{:S(2)}, u32[]{:S(2)}) %collective-permute-start) | collective-permute-done | bytes 131104 | tf_op jit(solution)/shard_map/ppermute | solution.py:305
  72.3 0.7 broadcast_select_fusion.state_ref
  72.9 2.0 advance.2
  74.9 4.2 %collective-permute-start.1 = (f32[64,512]{1,0:T(8,128)}, f32[64,512]{1,0:T(8,128)S(1)}, u32[]{:S(2)}, u32[]{:S(2)}) collective-permute-start(f32[64,512]{1,0:T(8,128)} %advance.2), channel_id=1, source_target_pairs={{0,4},{4,8},{8,12},{1,5},{5,9},{9,13},{2,6},{6,10},{10,14},{3,7},{... | collective-permute-start | bytes 393224 | tf_op jit(solution)/shard_map/ppermute | solution.py:305
  79.2 2.8 %collective-permute-done.1 = f32[64,512]{1,0:T(8,128)S(1)} collective-permute-done((f32[64,512]{1,0:T(8,128)}, f32[64,512]{1,0:T(8,128)S(1)}, u32[]{:S(2)}, u32[]{:S(2)}) %collective-permute-start.1) | collective-permute-done | bytes 131104 | tf_op jit(solution)/shard_map/ppermute | solution.py:305
  82.0 0.7 broadcast_select_fusion.1.state_ref
  82.7 2.0 advance.3
  84.6 4.2 %collective-permute-start.2 = (f32[64,512]{1,0:T(8,128)}, f32[64,512]{1,0:T(8,128)S(1)}, u32[]{:S(2)}, u32[]{:S(2)}) collective-permute-start(f32[64,512]{1,0:T(8,128)} %advance.3), channel_id=1, source_target_pairs={{0,4},{4,8},{8,12},{1,5},{5,9},{9,13},{2,6},{6,10},{10,14},{3,7},{... | collective-permute-start | bytes 393224 | tf_op jit(solution)/shard_map/ppermute | solution.py:305
  88.9 2.8 %collective-permute-done.2 = f32[64,512]{1,0:T(8,128)S(1)} collective-permute-done((f32[64,512]{1,0:T(8,128)}, f32[64,512]{1,0:T(8,128)S(1)}, u32[]{:S(2)}, u32[]{:S(2)}) %collective-permute-start.2) | collective-permute-done | bytes 131104 | tf_op jit(solution)/shard_map/ppermute | solution.py:305
  91.7 1.6 broadcast_select_fusion.2.state_ref
  93.3 6.6 %finish.1 = bf16[512,512]{1,0:T(8,128)(2,1)} custom-call(f32[512,512]{1,0:T(8,128)} %get-tuple-element.13.map_ref, f32[512,512]{1,0:T(8,128)} %get-tuple-element.14.own_ref, f32[64,512]{1,0:T(8,128)} %broadcast_select_fusion.2.state_ref, bf16[512,512]{1,0:T(8,128)(2,1)} %recept_ref.3, bf16[512,512]{1,0:T(8,128)(2,1)} %key_ref.3, bf16[512,512]{1,0:T(8,128)(2,1)} %value_ref.3, ...), custom_call_target="tpu_custom_call" | custom-call | flops 4000000000 | bytes 5242880 | tf_op jit(solution)/shard_map/finish/pallas_call | solution.py:307
  99.9 0.0 copy-done
  99.9 3.6 %convolution_convert_fusion = bf16[512,2048]{1,0:T(8,128)(2,1)} fusion(bf16[512,512]{1,0:T(8,128)(2,1)} %finish.1, bf16[512,2048]{1,0:T(8,128)(2,1)S(1)} %copy-done), kind=kOutput, calls=%fused_computation.8 | convolution fusion | flops 1074790400 | bytes 4718592 | tf_op jit(solution)/shard_map/dot_general | solution.py:369
  103.6 0.0 all-gather.10.cloned.1.call-done
  103.6 0.0 all-gather.12.cloned.1.call-done
  103.6 14.7 %all-gather.14.cloned.1.call-done = bf16[4,256,2048]{2,1,0:T(8,128)(2,1)} async-done(((bf16[1,256,2048]{2,1,0:T(8,128)(2,1)}), bf16[4,256,2048]{2,1,0:T(8,128)(2,1)}) %all-gather.14.cloned.1.call-update) | async-done | bytes 4194320 | tf_op jit(solution)/shard_map/all_gather | solution.py:354
  118.3 0.0 reduce-scatter.3.cloned.1.call-update
  118.3 0.0 all-gather.8.cloned.1.call-start
  118.5 0.1 copy.32
  118.6 33.3 %reduce-scatter.3.cloned.1.call-done = bf16[128,2048]{1,0:T(8,128)(2,1)} async-done(((bf16[512,2048]{1,0:T(8,128)(2,1)}), bf16[128,2048]{1,0:T(8,128)(2,1)}) %reduce-scatter.3.cloned.1.call-update) | async-done | bytes 524304 | tf_op jit(solution)/shard_map/reduce_scatter | solution.py:373
  151.9 1.3 multiply_reduce_fusion
  153.2 0.0 copy-done.4
  153.2 1.3 multiply_convert_fusion
  154.5 0.9 fusion.16
  155.3 0.0 all-gather.8.cloned.1.call-update
  155.3 0.2 reduce-scatter.5.cloned.1.call-start
  155.6 47.7 %all-gather.8.cloned.1.call-done = bf16[512,2176]{1,0:T(8,128)(2,1)} async-done(((bf16[128,2176]{1,0:T(8,128)(2,1)}), bf16[512,2176]{1,0:T(8,128)(2,1)}) %all-gather.8.cloned.1.call-update) | async-done | bytes 2228240 | tf_op jit(solution)/shard_map/all_gather | solution.py:396
  203.3 0.9 slice_convert_fusion
  204.3 0.3 fusion.18
  204.6 5.4 %fusion.5 = f32[4,256,512]{2,1,0:T(8,128)S(1)} fusion(bf16[4,1,2048,256]{3,2,0,1:T(8,128)(2,1)} %bitcast.48, bf16[512,2176]{1,0:T(8,128)(2,1)} %all-gather.8.cloned.1.call-done), kind=kOutput, calls=%fused_computation.6 | convolution fusion | flops 2147483648 | bytes 8388608 | tf_op jit(solution)/shard_map/rd,jdf->jrf/dot_general | solution.py:406
  210.0 2.7 fusion.9
  212.7 0.0 copy-done.9
  212.7 3.8 %fusion = bf16[512,2048]{1,0:T(8,128)(2,1)} fusion(bf16[4,512,256]{1,2,0:T(8,128)(2,1)S(1)} %fusion.9, bf16[4,1,256,2048]{3,2,0,1:T(8,128)(2,1)S(1)} %bitcast.50, f32[512]{0:T(512)S(1)} %fusion.18), kind=kOutput, calls=%fused_computation.1 | convolution fusion | flops 2149580800 | bytes 7342080 | tf_op jit(solution)/shard_map/jrf,jfd->rd/dot_general | solution.py:413
  216.5 0.0 reduce-scatter.5.cloned.1.call-update
  216.5 42.6 %reduce-scatter.5.cloned.1.call-done = bf16[128,2048]{1,0:T(8,128)(2,1)} async-done(((bf16[512,2048]{1,0:T(8,128)(2,1)}), bf16[128,2048]{1,0:T(8,128)(2,1)}) %reduce-scatter.5.cloned.1.call-update) | async-done | bytes 524304 | tf_op jit(solution)/shard_map/reduce_scatter | solution.py:418
  259.0 2.1 add_convert_fusion
  (20 shorter events, 0.1 us)
Async XLA Ops:
  6.5 93.4 %copy-start = (bf16[512,2048]{1,0:T(8,128)(2,1)S(1)}, bf16[512,2048]{1,0:T(8,128)(2,1)}, u32[]{:S(2)}) copy-start(bf16[512,2048]{1,0:T(8,128)(2,1)} %param.30) | copy-start | bytes 6291460
  6.5 2.3 copy-start.3
  6.5 97.1 %all-gather.10.cloned.1.call-start = ((), (), s32[]{:S(2)}) async-start(), calls=%async_computation.5 | async-start | bytes 5242880 | tf_op jit(solution)/shard_map/all_gather | solution.py:352
  7.3 96.4 %all-gather.12.cloned.1.call-start = ((), (), s32[]{:S(2)}) async-start(), calls=%async_computation.6 | async-start | bytes 5242880 | tf_op jit(solution)/shard_map/all_gather | solution.py:353
  8.0 110.3 %all-gather.14.cloned.1.call-start = ((), (), s32[]{:S(2)}) async-start(), calls=%async_computation.7 | async-start | bytes 5242880 | tf_op jit(solution)/shard_map/all_gather | solution.py:354
  8.7 143.1 %reduce-scatter.3.cloned.1.call-start = ((), (), s32[]{:S(2)}) async-start(), calls=%async_computation.2 | async-start | bytes 2621440 | tf_op jit(solution)/shard_map/reduce_scatter | solution.py:373
  64.2 8.0 %collective-permute-start = (f32[64,512]{1,0:T(8,128)}, f32[64,512]{1,0:T(8,128)S(1)}, u32[]{:S(2)}, u32[]{:S(2)}) collective-permute-start(f32[64,512]{1,0:T(8,128)} %get-tuple-element.15.added_ref), channel_id=1, source_target_pairs={{0,4},{4,8},{8,12},{1,5},{5,9},{9,13},{2,6},{6,10},{10,14},{3,7},{... | collective-permute-start | bytes 393224 | tf_op jit(solution)/shard_map/ppermute | solution.py:305
  74.9 7.1 %collective-permute-start.1 = (f32[64,512]{1,0:T(8,128)}, f32[64,512]{1,0:T(8,128)S(1)}, u32[]{:S(2)}, u32[]{:S(2)}) collective-permute-start(f32[64,512]{1,0:T(8,128)} %advance.2), channel_id=1, source_target_pairs={{0,4},{4,8},{8,12},{1,5},{5,9},{9,13},{2,6},{6,10},{10,14},{3,7},{... | collective-permute-start | bytes 393224 | tf_op jit(solution)/shard_map/ppermute | solution.py:305
  84.6 7.1 %collective-permute-start.2 = (f32[64,512]{1,0:T(8,128)}, f32[64,512]{1,0:T(8,128)S(1)}, u32[]{:S(2)}, u32[]{:S(2)}) collective-permute-start(f32[64,512]{1,0:T(8,128)} %advance.3), channel_id=1, source_target_pairs={{0,4},{4,8},{8,12},{1,5},{5,9},{9,13},{2,6},{6,10},{10,14},{3,7},{... | collective-permute-start | bytes 393224 | tf_op jit(solution)/shard_map/ppermute | solution.py:305
  103.6 14.8 %copy-start.6 = (f32[128,2]{0,1:T(2,128)S(1)}, f32[128,2]{0,1:T(2,128)}, u32[]{:S(2)}) copy-start(f32[128,2]{0,1:T(2,128)} %param.34) | copy-start | bytes 3076
  103.6 14.8 %copy-start.7 = (s32[128,2]{0,1:T(2,128)S(1)}, s32[128,2]{0,1:T(2,128)}, u32[]{:S(2)}) copy-start(s32[128,2]{0,1:T(2,128)} %param.33) | copy-start | bytes 3076
  103.6 48.3 %copy-start.1 = (bf16[128,2048]{1,0:T(8,128)(2,1)S(1)}, bf16[128,2048]{1,0:T(8,128)(2,1)}, u32[]{:S(2)}) copy-start(bf16[128,2048]{1,0:T(8,128)(2,1)} %param.31) | copy-start | bytes 1572868
  103.6 49.6 %copy-start.4 = (f32[2048]{0:T(1024)S(1)}, f32[2048]{0:T(1024)}, u32[]{:S(2)}) copy-start(f32[2048]{0:T(1024)} %param.32) | copy-start | bytes 24580
  118.3 85.0 %all-gather.8.cloned.1.call-start = ((), (), s32[]{:S(2)}) async-start(), calls=%async_computation.3 | async-start | bytes 2785280 | tf_op jit(solution)/shard_map/all_gather | solution.py:396
  155.3 103.7 %reduce-scatter.5.cloned.1.call-start = ((), (), s32[]{:S(2)}) async-start(), calls=%async_computation.4 | async-start | bytes 2621440 | tf_op jit(solution)/shard_map/reduce_scatter | solution.py:418
  204.6 5.4 %copy-start.5 = (bf16[512,2176]{1,0:T(8,128)(2,1)S(1)}, bf16[512,2176]{1,0:T(8,128)(2,1)}, u32[]{:S(2)}) copy-start(bf16[512,2176]{1,0:T(8,128)(2,1)} %all-gather.8.cloned.1.call-done) | copy-start | bytes 6684676
  204.6 5.4 %copy-start.8 = (bf16[4,2048,256]{2,1,0:T(8,128)(2,1)S(1)}, bf16[4,2048,256]{2,1,0:T(8,128)(2,1)}, u32[]{:S(2)}) copy-start(bf16[4,2048,256]{2,1,0:T(8,128)(2,1)} %all-gather.12.cloned.1.call-done) | copy-start | bytes 12582916
  210.0 2.7 %copy-start.9 = (bf16[4,256,2048]{2,1,0:T(8,128)(2,1)S(1)}, bf16[4,256,2048]{2,1,0:T(8,128)(2,1)}, u32[]{:S(2)}) copy-start(bf16[4,256,2048]{2,1,0:T(8,128)(2,1)} %all-gather.14.cloned.1.call-done) | copy-start | bytes 12582916
  216.5 42.6 %copy-start.2 = (bf16[128,2048]{1,0:T(8,128)(2,1)S(1)}, bf16[128,2048]{1,0:T(8,128)(2,1)}, u32[]{:S(2)}) copy-start(bf16[128,2048]{1,0:T(8,128)(2,1)} %reduce-scatter.3.cloned.1.call-done) | copy-start | bytes 1572868
Sparse Core Ops, SparseCore 0:
  8.9 37.3 all-gather.9
  47.8 34.3 all-gather.11
  83.8 34.4 all-gather.13
  120.7 31.1 reduce-scatter.2
  155.5 47.8 all-gather.7
  216.6 42.3 reduce-scatter.4
where the time goes:
time: 269 us; the launch traced here: 268 us
  waiting for transfers between devices  149 us (55%)
  Pallas kernels  65.2 us (24%)
  matrix products  15.5 us (6%)
  starting transfers between devices  13.8 us (5%)
  between operations  13.7 us (5%)
  other arithmetic  9.69 us (4%)
    pallas_call x1, Pallas kernels, mixer(): pl.pallas_call(functools.partial(chunk_kernel, head_width), grid=(length...  54.6 us
    all_gather x1, waiting for transfers between devices, local(): lax.all_gather(jnp.concatenate([ffn_in, extra], axis=1), 'sp', axis=0, ti...  47.7 us
    reduce_scatter x1, waiting for transfers between devices, local(): lax.psum_scatter(total.astype(jnp.bfloat16), 'sp', scatter_dimension=0, t...  42.6 us
    reduce_scatter x1, waiting for transfers between devices, local(): proj = lax.psum_scatter(part, 'tp', scatter_dimension=0, tiled=True)  33.3 us
    all_gather x1, waiting for transfers between devices, local(): downs = lax.all_gather(down_weight_experts, 'tp', axis=0)  14.7 us
    ppermute x3, starting transfers between devices, mixer(): got = lax.ppermute(sent, 'sp', [(i, i + 1) for i in range(axis_size - 1)])  13.4 us
    ppermute x3, waiting for transfers between devices, mixer(): got = lax.ppermute(sent, 'sp', [(i, i + 1) for i in range(axis_size - 1)])  8.65 us
    pallas_call x1, Pallas kernels, mixer(): pl.pallas_call(functools.partial(finish_kernel, head_width), grid=(length...  6.63 us
  transfers between devices with their start and end apart: 9, of which 7 were waited for; matrix products, arithmetic and copies ran while one was open for 3% of the time, Pallas kernels for 24%

commit v1 on v0

--- a/solution.py
+++ b/solution.py
@@ -14,7 +14,33 @@
 NORM_EPS = 1e-06
 NN = (((1,), (0,)), ((), ()))
 NT = (((1,), (1,)), ((), ()))
-TN = (((0,), (0,)), ((), ()))
+MESH = pl.DeviceIdType.MESH
+VMEM_LIMIT = 60 * 1024 * 1024
+
+
+def peer(**coords):
+    return tuple(coords.get(name, lax.axis_index(name)) for name in ("grp", "sp", "tp"))
+
+
+def tp_peers():
+    place = lax.axis_index("tp")
+    chip, core = place // 2, place % 2
+    return 2 * chip + 1 - core, 2 * (1 - chip) + core, 2 * (1 - chip) + 1 - core
+
+
+def remote(src, dst, send_sem, recv_sem, device):
+    return pltpu.make_async_remote_copy(
+        src_ref=src,
+        dst_ref=dst,
+        send_sem=send_sem,
+        recv_sem=recv_sem,
+        device_id=device,
+        device_id_type=MESH,
+    )
+
+
+def greet(barrier, device):
+    pl.semaphore_signal(barrier, inc=1, device_id=device, device_id_type=MESH)
 
 
 def halves(x):
@@ -45,6 +71,147 @@
     return lax.dot_general(
         high, mask, NN, preferred_element_type=jnp.float32
     ) + lax.dot_general(low, mask, NN, preferred_element_type=jnp.float32)
+
+
+class Gather:
+    def __init__(self, own, full, sems):
+        self.own, self.full = own, full
+        (
+            self.core_send,
+            self.core_recv,
+            self.chip_send,
+            self.chip_recv,
+            self.swap_send,
+            self.swap_recv,
+            self.pass_send,
+            self.pass_recv,
+        ) = sems
+        near, far, _ = tp_peers()
+        self.group = lax.axis_index("grp")
+        self.near, self.far = peer(tp=near), peer(tp=far)
+        self.twin = peer(grp=1 - self.group)
+
+    def enter(self, others):
+        barrier = pltpu.get_barrier_semaphore()
+        for device in (self.near, self.far, self.twin):
+            greet(barrier, device)
+        pl.semaphore_wait(barrier, 3 + others(barrier))
+
+    def half(self, ref, which):
+        rows = ref.shape[0] // 2
+        return ref.at[pl.ds(pl.multiple_of(which * rows, rows), rows)]
+
+    def core_copy(self, k):
+        return remote(
+            self.own[k], self.full[k].at[0], self.core_send.at[k], self.core_recv.at[k], self.near
+        )
+
+    def chip_copy(self, k):
+        return remote(
+            self.half(self.own[k], self.group),
+            self.half(self.full[k].at[1], self.group),
+            self.chip_send.at[k],
+            self.chip_recv.at[k],
+            self.far,
+        )
+
+    def swap_copy(self, k):
+        piece = self.half(self.full[k].at[1], self.group)
+        return remote(piece, piece, self.swap_send.at[k], self.swap_recv.at[k], self.twin)
+
+    def pass_copy(self, k, swapped):
+        which = 1 - self.group if swapped else self.group
+        slot = 2 * k + swapped
+        return remote(
+            self.half(self.full[k].at[1], which),
+            self.half(self.full[k].at[2], which),
+            self.pass_send.at[slot],
+            self.pass_recv.at[slot],
+            self.near,
+        )
+
+    def begin(self):
+        for k in range(3):
+            self.chip_copy(k).start()
+        for k in range(3):
+            self.core_copy(k).start()
+
+    def arrive_chip(self, k):
+        self.chip_copy(k).wait_recv()
+        self.swap_copy(k).start()
+        self.pass_copy(k, 0).start()
+
+    def arrive_swap(self, k):
+        piece = self.half(self.full[k].at[1], 1 - self.group)
+        remote(piece, piece, self.swap_send.at[k], self.swap_recv.at[k], self.twin).wait_recv()
+        self.pass_copy(k, 1).start()
+
+    def middle(self, k):
+        self.arrive_chip(k)
+        if k > 0:
+            self.arrive_swap(k - 1)
+
+    def end(self):
+        self.arrive_swap(2)
+        for k in range(3):
+            self.core_copy(k).wait()
+            self.chip_copy(k).wait_send()
+            self.swap_copy(k).wait_send()
+            for swapped in range(2):
+                self.pass_copy(k, swapped).wait()
+
+
+class Spread:
+    def __init__(self, own, full, send, recv, local):
+        self.own, self.full, self.send, self.recv, self.local = own, full, send, recv, local
+        self.count = lax.axis_size("sp")
+        self.place = lax.axis_index("sp")
+
+    def greet(self, barrier):
+        def one(ahead, carry):
+            greet(barrier, peer(sp=(self.place + ahead) % self.count))
+            return carry
+
+        lax.fori_loop(1, self.count, one, 0)
+        return self.count - 1
+
+    def copy(self, ahead):
+        return remote(
+            self.own,
+            self.full.at[self.place],
+            self.send.at[ahead - 1],
+            self.recv.at[self.place],
+            peer(sp=(self.place + ahead) % self.count),
+        )
+
+    def arrival(self, ahead):
+        source = (self.place + self.count - ahead) % self.count
+        return remote(
+            self.own,
+            self.full.at[source],
+            self.send.at[ahead - 1],
+            self.recv.at[source],
+            peer(sp=source),
+        )
+
+    def begin(self):
+        pltpu.make_async_copy(self.own, self.full.at[self.place], self.local).start()
+
+        def one(ahead, carry):
+            self.copy(ahead).start()
+            return carry
+
+        lax.fori_loop(1, self.count, one, 0)
+
+    def end(self):
+        pltpu.make_async_copy(self.own, self.full.at[self.place], self.local).wait()
+
+        def one(ahead, carry):
+            self.copy(ahead).wait_send()
+            self.arrival(ahead).wait_recv()
+            return carry
+
+        lax.fori_loop(1, self.count, one, 0)
 
 
 def chunk_kernel(
@@ -57,11 +224,48 @@
     offset_ref,
     decay_bias_ref,
     rate_bias_ref,
+    share_ref,
+    gate_ref,
+    up_ref,
+    down_ref,
     map_ref,
     own_ref,
     transit_ref,
     added_ref,
+    shares_ref,
+    gates_ref,
+    ups_ref,
+    downs_ref,
+    core_send,
+    core_recv,
+    chip_send,
+    chip_recv,
+    swap_send,
+    swap_recv,
+    pass_send,
+    pass_recv,
+    share_send,
+    share_recv,
+    local_sem,
 ):
+    weights = Gather(
+        (gate_ref, up_ref, down_ref),
+        (gates_ref, ups_ref, downs_ref),
+        (core_send, core_recv, chip_send, chip_recv, swap_send, swap_recv, pass_send, pass_recv),
+    )
+    shares = Spread(share_ref, shares_ref, share_send, share_recv, local_sem)
+    step = pl.program_id(0)
+    last_step = pl.num_programs(0) - 1
+
+    @pl.when(step == 0)
+    def _():
+        weights.enter(shares.greet)
+        weights.begin()
+        shares.begin()
+
+    for number in range(1, 4):
+        pl.when(step == number)(functools.partial(weights.middle, number - 1))
+
     span = head_width
     wide_mask = block_mask(head_width)
     mask = wide_mask.astype(jnp.bfloat16)
@@ -205,127 +409,404 @@
         transit_ref[:, cols] = moved[:span]
         added_ref[:, cols] = moved[span:] + added
 
-
-def advance_kernel(head_width, state_ref, transit_ref, added_ref, out_ref):
-    mask = block_mask(head_width).astype(jnp.bfloat16)
-    for group in range(state_ref.shape[1] // LANES):
+    @pl.when(step == last_step)
+    def _():
+        weights.end()
+        shares.end()
+
+
+def mixed_rows(head_width, rows, state, refs, mask):
+    map_ref, own_ref, recept_ref, key_ref, value_ref, gate_ref, gain_ref, self_ref = refs
+    parts = []
+    for group in range(map_ref.shape[1] // LANES):
         cols = slice(group * LANES, (group + 1) * LANES)
-        out_ref[:, cols] = added_ref[:, cols] + product(
-            halves(state_ref[:, cols]), spread_blocks(transit_ref[:, cols], mask), NN
-        )
-
-
-def finish_kernel(
+        read = own_ref[rows, cols] + product(
+            halves(map_ref[rows, cols]), spread_blocks(state[group], mask), NT
+        )
+        off = read - head_sum(read, mask) * (1.0 / head_width)
+        spread = head_sum(off * off, mask) * (1.0 / head_width)
+        normed = off * lax.rsqrt(spread + GROUP_EPS) * gain_ref[:, cols]
+        value = value_ref[rows, cols].astype(jnp.float32)
+        own = (
+            head_sum(
+                recept_ref[rows, cols].astype(jnp.float32)
+                * key_ref[rows, cols].astype(jnp.float32)
+                * self_ref[:, cols],
+                mask,
+            )
+            * value
+        )
+        parts.append(
+            ((normed + own) * gate_ref[rows, cols].astype(jnp.float32)).astype(jnp.bfloat16)
+        )
+    return parts
+
+
+def middle_kernel(
     head_width,
     map_ref,
     own_ref,
-    state_ref,
+    transit_ref,
+    added_ref,
     recept_ref,
     key_ref,
     value_ref,
     gate_ref,
     gain_ref,
     self_ref,
+    out_weight_ref,
+    residual_ref,
+    norm_gain_ref,
+    stream_ref,
+    features_ref,
+    state_ref,
+    onward_ref,
+    core_out,
+    core_in,
+    chip_out,
+    chip_in,
+    state_send,
+    state_recv,
+    core_send,
+    core_recv,
+    chip_send,
+    chip_recv,
+):
+    place, count = lax.axis_index("sp"), lax.axis_size("sp")
+    near, far, cross = tp_peers()
+    mine = lax.axis_index("tp")
+    groups = map_ref.shape[1] // LANES
+    rows = residual_ref.shape[0]
+    parts = chip_out.shape[0]
+    mask = block_mask(head_width).astype(jnp.bfloat16)
+    barrier = pltpu.get_barrier_semaphore()
+    greet(barrier, peer(tp=near))
+    greet(barrier, peer(tp=far))
+    ahead, behind = peer(sp=(place + 1) % count), peer(sp=(place + count - 1) % count)
+
+    @pl.when(place > 0)
+    def _():
+        greet(barrier, behind)
+
+    @pl.when(place < count - 1)
+    def _():
+        greet(barrier, ahead)
+
+    pl.semaphore_wait(
+        barrier, 2 + jnp.where(place > 0, 1, 0) + jnp.where(place < count - 1, 1, 0)
+    )
+
+    def state_copy(group):
+        return remote(
+            onward_ref.at[group],
+            state_ref.at[group],
+            state_send.at[group],
+            state_recv.at[group],
+            ahead,
+        )
+
+    @pl.when(place == 0)
+    def _():
+        for group in range(groups):
+            cols = slice(group * LANES, (group + 1) * LANES)
+            state_ref[group] = jnp.zeros_like(state_ref[group])
+            onward_ref[group] = added_ref[:, cols]
+            state_copy(group).start()
+
+    @pl.when(place > 0)
+    def _():
+        for group in range(groups):
+            cols = slice(group * LANES, (group + 1) * LANES)
+            state_copy(group).wait_recv()
+
+            @pl.when(place < count - 1)
+            def _(group=group, cols=cols):
+                onward_ref[group] = added_ref[:, cols] + product(
+                    halves(state_ref[group]), spread_blocks(transit_ref[:, cols], mask), NN
+                )
+                state_copy(group).start()
+
+    refs = (map_ref, own_ref, recept_ref, key_ref, value_ref, gate_ref, gain_ref, self_ref)
+
+    def partial(owner, part):
+        size = rows // parts
+        at = pl.ds(pl.multiple_of(owner * rows + part * size, size), size)
+        total = None
+        for group, mixed in enumerate(
+            mixed_rows(head_width, at, [state_ref[g] for g in range(groups)], refs, mask)
+        ):
+            term = lax.dot_general(
+                mixed,
+                out_weight_ref[group * LANES : (group + 1) * LANES],
+                NN,
+                preferred_element_type=jnp.float32,
+            )
+            total = term if total is None else total + term
+        return total
+
+    def core_copy(which, part):
+        slot = which * parts + part
+        return remote(
+            core_out.at[slot],
+            core_in.at[slot],
+            core_send.at[slot],
+            core_recv.at[slot],
+            peer(tp=near),
+        )
+
+    def chip_copy(part):
+        return remote(
+            chip_out.at[part],
+            chip_in.at[part],
+            chip_send.at[part],
+            chip_recv.at[part],
+            peer(tp=far),
+        )
+
+    for part in range(parts):
+        core_out[part] = partial(cross, part)
+        core_copy(0, part).start()
+        own = partial(far, part)
+        core_copy(0, part).wait_recv()
+        chip_out[part] = (own + core_in[part]).astype(jnp.bfloat16)
+        chip_copy(part).start()
+    for part in range(parts):
+        core_out[parts + part] = partial(near, part)
+        core_copy(1, part).start()
+        own = partial(mine, part)
+        core_copy(1, part).wait_recv()
+        size = rows // parts
+        stream_ref[part * size : (part + 1) * size] = (
+            residual_ref[part * size : (part + 1) * size].astype(jnp.float32)
+            + own
+            + core_in[parts + part]
+        )
+    for part in range(parts):
+        size = rows // parts
+        at = slice(part * size, (part + 1) * size)
+        chip_copy(part).wait_recv()
+        stream = stream_ref[at] + chip_in[part].astype(jnp.float32)
+        stream_ref[at] = stream
+        features_ref[at] = (
+            stream
+            * lax.rsqrt(jnp.mean(stream * stream, axis=-1, keepdims=True) + NORM_EPS)
+            * norm_gain_ref[...]
+        ).astype(jnp.bfloat16)
+
+    @pl.when(place < count - 1)
+    def _():
+        for group in range(groups):
+            state_copy(group).wait_send()
+
+    for part in range(parts):
+        core_copy(0, part).wait_send()
+        core_copy(1, part).wait_send()
+        chip_copy(part).wait_send()
+
+
+def expert_kernel(
+    pieces,
+    lag,
+    features_ref,
+    stream_ref,
+    shares_ref,
+    gate_ref,
+    up_ref,
+    down_ref,
+    gates_ref,
+    ups_ref,
+    downs_ref,
     out_ref,
+    gate_all,
+    up_all,
+    down_all,
+    blocks,
+    result,
+    from_right,
+    from_left,
+    to_left,
+    to_right,
+    load_sem,
+    gather_send,
+    gather_recv,
+    sum_send,
+    sum_recv,
 ):
-    mask = block_mask(head_width).astype(jnp.bfloat16)
-    for group in range(map_ref.shape[1] // LANES):
-        cols = slice(group * LANES, (group + 1) * LANES)
-        read = own_ref[:, cols] + product(
-            halves(map_ref[:, cols]), spread_blocks(state_ref[:, cols], mask), NT
-        )
-        off = read - head_sum(read, mask) * (1.0 / head_width)
-        spread = head_sum(off * off, mask) * (1.0 / head_width)
-        normed = off * lax.rsqrt(spread + GROUP_EPS) * gain_ref[:, cols]
-        own = head_sum(
-            recept_ref[:, cols].astype(jnp.float32)
-            * key_ref[:, cols].astype(jnp.float32)
-            * self_ref[:, cols],
-            mask,
-        ) * value_ref[:, cols].astype(jnp.float32)
-        out_ref[:, cols] = ((normed + own) * gate_ref[:, cols].astype(jnp.float32)).astype(
-            jnp.bfloat16
-        )
-
-
-def mixer(
-    recept,
-    key_input,
-    value_input,
-    output_gate_input,
-    decay_input_part,
-    correction_rate_input,
-    head_decay_offset,
-    decay_fixed_bias,
-    correction_rate_bias,
-    head_norm_gain,
-    self_term_weight,
-    axis_size,
-):
-    length, width = recept.shape
-    heads = head_decay_offset.shape[1]
-    head_width = width // heads
-    rows = 2 * SPAN
-    by_rows = pl.BlockSpec((rows, width), lambda i: (i, 0))
-    fixed = pl.BlockSpec((1, width), lambda i: (0, 0))
-    states = pl.BlockSpec((head_width, width), lambda i: (0, 0))
-    wide = jax.ShapeDtypeStruct((length, width), jnp.float32)
-    small = jax.ShapeDtypeStruct((head_width, width), jnp.float32)
-    params = pltpu.CompilerParams(dimension_semantics=("arbitrary",))
-    read_map, read_own, transit, added = pl.pallas_call(
-        functools.partial(chunk_kernel, head_width),
-        grid=(length // rows,),
-        in_specs=[by_rows] * 5
-        + [pl.BlockSpec((rows, heads), lambda i: (i, 0)), fixed, fixed],
-        out_specs=[by_rows, by_rows, states, states],
-        out_shape=[wide, wide, small, small],
-        compiler_params=params,
-        cost_estimate=pl.CostEstimate(
-            flops=30_000_000_000, bytes_accessed=8 * length * width, transcendentals=0
+    place, count = lax.axis_index("sp"), lax.axis_size("sp")
+    left, right = peer(sp=(place + count - 1) % count), peer(sp=(place + 1) % count)
+    has_left, has_right = place > 0, place < count - 1
+    size = features_ref.shape[0] // pieces
+    loads = []
+    for k, (own, rest, full) in enumerate(
+        ((gate_ref, gates_ref, gate_all), (up_ref, ups_ref, up_all), (down_ref, downs_ref, down_all))
+    ):
+        loads.append(pltpu.make_async_copy(own, full.at[0], load_sem.at[2 * k]))
+        loads.append(
+            pltpu.make_async_copy(rest, full.at[pl.ds(1, rest.shape[0])], load_sem.at[2 * k + 1])
+        )
+    for load in loads:
+        load.start()
+    barrier = pltpu.get_barrier_semaphore()
+    for there, device in ((has_left, left), (has_right, right)):
+        pl.when(there)(functools.partial(greet, barrier, device))
+    pl.semaphore_wait(barrier, jnp.where(has_left, 1, 0) + jnp.where(has_right, 1, 0))
+
+    def gather_copy(source, block, piece, way):
+        return remote(
+            source,
+            blocks.at[block, piece],
+            gather_send.at[way, block, piece],
+            gather_recv.at[block, piece],
+            right if way else left,
+        )
+
+    def sum_copy(block, piece, way):
+        out, into = (to_right, from_left) if way else (to_left, from_right)
+        return remote(
+            out.at[block, piece],
+            into.at[block, piece],
+            sum_send.at[way, block, piece],
+            sum_recv.at[way, block, piece],
+            right if way else left,
+        )
+
+    for piece in range(pieces):
+        mine = features_ref.at[pl.ds(piece * size, size)]
+        for way, there in ((0, has_left), (1, has_right)):
+            pl.when(there)(lambda: gather_copy(mine, place, piece, way).start())
+
+    def apply(features, block, piece):
+        total = None
+        for j in range(gate_all.shape[0]):
+            gated = lax.dot_general(
+                features, gate_all[j], NN, preferred_element_type=jnp.float32
+            )
+            upward = lax.dot_general(features, up_all[j], NN, preferred_element_type=jnp.float32)
+            hidden = (jax.nn.silu(gated) * upward).astype(jnp.bfloat16)
+            term = lax.dot_general(hidden, down_all[j], NN, preferred_element_type=jnp.float32)
+            total = term if total is None else total + term
+        weights = shares_ref[block, pl.ds(pl.multiple_of(piece * size, size), size)]
+        lanes = lax.broadcasted_iota(jnp.int32, weights.shape, 1)
+        share = jnp.sum(jnp.where(lanes == place, weights, 0.0), axis=1, keepdims=True)
+        result[block, piece] = total * share
+
+    for load in loads:
+        load.wait()
+
+    def own_piece(piece, carry):
+        apply(
+            features_ref[pl.ds(pl.multiple_of(piece * size, size), size)], place, piece
+        )
+        return carry
+
+    lax.fori_loop(0, pieces, own_piece, 0)
+
+    def slot(time, carry):
+        distance, piece = time // pieces + 1, time % pieces
+        for way, block, there, onward in (
+            (1, place - distance, place - distance >= 0, has_right),
+            (0, place + distance, place + distance < count, has_left),
+        ):
+
+            @pl.when(there)
+            def _(way=way, block=block, onward=onward):
+                landed = blocks.at[block, piece]
+                gather_copy(landed, block, piece, way).wait_recv()
+                pl.when(onward)(lambda: gather_copy(landed, block, piece, way).start())
+
+        for block, there in (
+            (place - distance, place - distance >= 0),
+            (place + distance, place + distance < count),
+        ):
+
+            @pl.when(there)
+            def _(block=block):
+                apply(blocks[block, piece], block, piece)
+
+        for way, hops, first, step, more, into, out in (
+            (0, count - 1 - place, count - 2, -1, has_right, from_right, to_left),
+            (1, place, 1, 1, has_left, from_left, to_right),
+        ):
+            turn = time - lag * hops
+            block = first + step * (turn // pieces)
+            part = turn % pieces
+            passed = (place - block) * (1 - 2 * way)
+            valid = (turn >= 0) & (block >= 0) & (block < count) & (passed >= 0)
+
+            @pl.when(valid & more)
+            def _(way=way, block=block, part=part, into=into):
+                sum_copy(block, part, way).wait_recv()
+                result[block, part] = result[block, part] + into[block, part].astype(jnp.float32)
+
+            @pl.when(valid & (passed > 0))
+            def _(way=way, block=block, part=part, out=out):
+                out[block, part] = result[block, part].astype(jnp.bfloat16)
+                sum_copy(block, part, way).start()
+
+        return carry
+
+    lax.fori_loop(0, (count - 1) * pieces + lag * (count - 1), slot, 0)
+    for piece in range(pieces):
+        at = slice(piece * size, (piece + 1) * size)
+        out_ref[at] = (stream_ref[at] + result[place, piece]).astype(out_ref.dtype)
+
+    def drain(block, carry):
+        for piece in range(pieces):
+            landed = blocks.at[block, piece]
+            for way, gathers, sums in (
+                (0, has_left & (block >= place), has_left & (block < place)),
+                (1, has_right & (block <= place), has_right & (block > place)),
+            ):
+                pl.when(gathers)(
+                    lambda: gather_copy(landed, block, piece, way).wait_send()
+                )
+                pl.when(sums)(lambda: sum_copy(block, piece, way).wait_send())
+        return carry
+
+    lax.fori_loop(0, count, drain, 0)
+
+
+def shares_of(routed_expert_index, routed_expert_weight, experts):
+    ids = jnp.arange(experts, dtype=jnp.int32)
+    shares = jnp.sum(
+        jnp.where(
+            routed_expert_index[:, :, None] == ids, routed_expert_weight[:, :, None], 0.0
         ),
-        name="chunks",
-    )(
-        recept,
-        key_input,
-        value_input,
-        decay_input_part,
-        correction_rate_input,
-        head_decay_offset,
-        decay_fixed_bias[None],
-        correction_rate_bias[None],
+        axis=1,
     )
+    return jnp.pad(shares, ((0, 0), (0, -experts % 128)))
+
+
+def experts_by_collectives(features, stream, shares, gates, ups, downs):
+    features = lax.all_gather(features, "sp", axis=0, tiled=True)
+    shares = shares.reshape(-1, shares.shape[-1])
     place = lax.axis_index("sp")
-    state = jnp.zeros_like(added)
-    for lap in range(axis_size - 1):
-        sent = added
-        if lap > 0:
-            sent = pl.pallas_call(
-                functools.partial(advance_kernel, head_width), out_shape=small, name="advance"
-            )(state, transit, added)
-        got = lax.ppermute(sent, "sp", [(i, i + 1) for i in range(axis_size - 1)])
-        state = jnp.where(place == lap + 1, got, state)
-    return pl.pallas_call(
-        functools.partial(finish_kernel, head_width),
-        grid=(length // rows,),
-        in_specs=[by_rows, by_rows, states] + [by_rows] * 4 + [fixed, fixed],
-        out_specs=by_rows,
-        out_shape=jax.ShapeDtypeStruct((length, width), jnp.bfloat16),
-        compiler_params=params,
-        cost_estimate=pl.CostEstimate(
-            flops=4_000_000_000, bytes_accessed=20 * length * width, transcendentals=0
-        ),
-        name="finish",
-    )(
-        read_map,
-        read_own,
-        state,
-        recept,
-        key_input,
-        value_input,
-        output_gate_input,
-        head_norm_gain[None],
-        self_term_weight[None],
-    )
+    lanes = jnp.arange(shares.shape[1], dtype=jnp.int32)
+    share = jnp.sum(jnp.where(lanes[None, :] == place, shares, 0.0), axis=1, keepdims=True)
+    depth = features.shape[1]
+
+    def some_rows(operands):
+        features, share = operands
+        total = None
+        for gate, up, down in zip(gates, ups, downs):
+            for j in range(gate.shape[0]):
+                gated = jnp.dot(features, gate[j], preferred_element_type=jnp.float32)
+                upward = jnp.dot(features, up[j], preferred_element_type=jnp.float32)
+                hidden = (jax.nn.silu(gated) * upward).astype(jnp.bfloat16)
+                term = jnp.dot(hidden, down[j], preferred_element_type=jnp.float32)
+                total = term if total is None else total + term
+        return (total * share).astype(jnp.bfloat16)
+
+    rows = stream.shape[0]
+    total = lax.map(
+        some_rows, (features.reshape(-1, rows, depth), share.reshape(-1, rows, 1))
+    ).reshape(-1, depth)
+    weighted = lax.psum_scatter(total, "sp", scatter_dimension=0, tiled=True)
+    return (stream + weighted.astype(jnp.float32)).astype(jnp.bfloat16)
+
+
+PIECES = 2
+LAG = 2
 
 
 def local(
@@ -349,76 +830,153 @@
     up_weight_experts,
     down_weight_experts,
 ):
-    gates = lax.all_gather(gate_weight_experts, "tp", axis=0)
-    ups = lax.all_gather(up_weight_experts, "tp", axis=0)
-    downs = lax.all_gather(down_weight_experts, "tp", axis=0)
-    attention_result = mixer(
+    count = lax.axis_size("sp")
+    experts = gate_weight_experts.shape[0] * count
+    assert lax.axis_size("tp") == 4 and lax.axis_size("grp") == 2
+    assert gate_weight_experts.shape[0] == 1
+    length, width = recept.shape
+    heads = head_decay_offset.shape[1]
+    head_width = width // heads
+    rows = 2 * SPAN
+    own_rows, depth = residual.shape
+    shares = shares_of(routed_expert_index, routed_expert_weight, experts)
+    gate, up, down = gate_weight_experts[0], up_weight_experts[0], down_weight_experts[0]
+    by_rows = pl.BlockSpec((rows, width), lambda i: (i, 0))
+    fixed = pl.BlockSpec((1, width), lambda i: (0, 0))
+    states = pl.BlockSpec((head_width, width), lambda i: (0, 0))
+    anywhere = pl.BlockSpec(memory_space=pl.ANY)
+    in_vmem = pl.BlockSpec(memory_space=pltpu.VMEM)
+    wide = jax.ShapeDtypeStruct((length, width), jnp.float32)
+    small = jax.ShapeDtypeStruct((head_width, width), jnp.float32)
+    dma = pltpu.SemaphoreType.DMA
+
+    def three(x):
+        return jax.ShapeDtypeStruct((3, *x.shape), x.dtype)
+
+    read_map, read_own, transit, added, all_shares, gates, ups, downs = pl.pallas_call(
+        functools.partial(chunk_kernel, head_width),
+        grid=(length // rows,),
+        in_specs=[by_rows] * 5
+        + [pl.BlockSpec((rows, heads), lambda i: (i, 0)), fixed, fixed]
+        + [anywhere] * 4,
+        out_specs=[by_rows, by_rows, states, states] + [anywhere] * 4,
+        out_shape=[
+            wide,
+            wide,
+            small,
+            small,
+            jax.ShapeDtypeStruct((count, *shares.shape), shares.dtype),
+            three(gate),
+            three(up),
+            three(down),
+        ],
+        scratch_shapes=[dma((3,))] * 6
+        + [dma((6,))] * 2
+        + [dma((count,)), dma((count,)), dma],
+        compiler_params=pltpu.CompilerParams(
+            dimension_semantics=("arbitrary",),
+            collective_id=0,
+            has_side_effects=True,
+            vmem_limit_bytes=32 * 1024 * 1024,
+        ),
+        cost_estimate=pl.CostEstimate(
+            flops=30_000_000_000, bytes_accessed=8 * length * width, transcendentals=0
+        ),
+        name="chunks",
+    )(
+        recept,
+        key_input,
+        value_input,
+        decay_input_part,
+        correction_rate_input,
+        head_decay_offset,
+        decay_fixed_bias[None],
+        correction_rate_bias[None],
+        shares,
+        gate,
+        up,
+        down,
+    )
+    groups = width // LANES
+    half = own_rows // PIECES
+    own_wide = jax.ShapeDtypeStruct((own_rows, depth), jnp.float32)
+    own_narrow = jax.ShapeDtypeStruct((own_rows, depth), jnp.bfloat16)
+    stream, features = pl.pallas_call(
+        functools.partial(middle_kernel, head_width),
+        in_specs=[in_vmem] * 13,
+        out_specs=[in_vmem] * 2,
+        out_shape=[own_wide, own_narrow],
+        scratch_shapes=[
+            pltpu.VMEM((groups, head_width, LANES), jnp.float32),
+            pltpu.VMEM((groups, head_width, LANES), jnp.float32),
+            pltpu.VMEM((2 * PIECES, half, depth), jnp.float32),
+            pltpu.VMEM((2 * PIECES, half, depth), jnp.float32),
+            pltpu.VMEM((PIECES, half, depth), jnp.bfloat16),
+            pltpu.VMEM((PIECES, half, depth), jnp.bfloat16),
+            dma((groups,)),
+            dma((groups,)),
+            dma((2 * PIECES,)),
+            dma((2 * PIECES,)),
+            dma((PIECES,)),
+            dma((PIECES,)),
+        ],
+        compiler_params=pltpu.CompilerParams(
+            collective_id=1, has_side_effects=True, vmem_limit_bytes=VMEM_LIMIT
+        ),
+        cost_estimate=pl.CostEstimate(
+            flops=8_000_000_000, bytes_accessed=20 * length * width, transcendentals=0
+        ),
+        name="middle",
+    )(
+        read_map,
+        read_own,
+        transit,
+        added,
         recept,
         key_input,
         value_input,
         output_gate_input,
-        decay_input_part,
-        correction_rate_input,
-        head_decay_offset,
-        decay_fixed_bias,
-        correction_rate_bias,
-        head_norm_gain,
-        self_term_weight,
-        lax.axis_size("sp"),
+        head_norm_gain[None],
+        self_term_weight[None],
+        output_weight_matrix,
+        residual,
+        feedforward_norm_gain[None],
     )
-    part = jnp.dot(
-        attention_result, output_weight_matrix, preferred_element_type=jnp.float32
-    ).astype(jnp.bfloat16)
-    part, gates, ups, downs = lax.optimization_barrier((part, gates, ups, downs))
-    proj = lax.psum_scatter(part, "tp", scatter_dimension=0, tiled=True)
-    stream = residual.astype(jnp.float32) + lax.optimization_barrier(proj).astype(jnp.float32)
-    ffn_in = (
-        stream
-        * lax.rsqrt(jnp.mean(stream * stream, axis=-1, keepdims=True) + NORM_EPS)
-        * feedforward_norm_gain
-    ).astype(jnp.bfloat16)
-    width = ffn_in.shape[1]
-    local_experts = gate_weight_experts.shape[0]
-    experts = local_experts * lax.axis_size("sp")
-    ids = jnp.arange(experts, dtype=jnp.int32)
-    shares = jnp.sum(
-        jnp.where(
-            routed_expert_index[:, :, None] == ids, routed_expert_weight[:, :, None], 0.0
+    if count > 4:
+        return experts_by_collectives(
+            features, stream, all_shares, (gate[None], gates), (up[None], ups), (down[None], downs)
+        )
+    flow = pltpu.VMEM((count, PIECES, half, depth), jnp.bfloat16)
+    both = dma((2, count, PIECES))
+    return pl.pallas_call(
+        functools.partial(expert_kernel, PIECES, LAG),
+        in_specs=[in_vmem] * 3 + [anywhere] * 6,
+        out_specs=in_vmem,
+        out_shape=own_narrow,
+        scratch_shapes=[
+            pltpu.VMEM((4, *gate.shape), gate.dtype),
+            pltpu.VMEM((4, *up.shape), up.dtype),
+            pltpu.VMEM((4, *down.shape), down.dtype),
+            flow,
+            pltpu.VMEM((count, PIECES, half, depth), jnp.float32),
+            flow,
+            flow,
+            flow,
+            flow,
+            dma((6,)),
+            both,
+            dma((count, PIECES)),
+            both,
+            both,
+        ],
+        compiler_params=pltpu.CompilerParams(
+            collective_id=2, has_side_effects=True, vmem_limit_bytes=VMEM_LIMIT
         ),
-        axis=1,
-    )
-    first = shares.astype(jnp.bfloat16)
-    rest = shares - first.astype(jnp.float32)
-    second = rest.astype(jnp.bfloat16)
-    third = (rest - second.astype(jnp.float32)).astype(jnp.bfloat16)
-    extra = jnp.concatenate([first, second, third], axis=1)
-    extra = jnp.pad(extra, ((0, 0), (0, -extra.shape[1] % 128)))
-    packed = lax.all_gather(
-        jnp.concatenate([ffn_in, extra], axis=1), "sp", axis=0, tiled=True
-    )
-    features = packed[:, :width]
-    tail = packed[:, width : width + 3 * experts].astype(jnp.float32)
-    shares = tail[:, :experts] + tail[:, experts : 2 * experts] + tail[:, 2 * experts :]
-    total = None
-    for own in range(local_experts):
-        expert = lax.axis_index("sp") * local_experts + own
-        share = jnp.sum(jnp.where(ids[None, :] == expert, shares, 0.0), axis=1, keepdims=True)
-        gated = jnp.einsum(
-            "rd,jdf->jrf", features, gates[:, own], preferred_element_type=jnp.float32
-        )
-        upward = jnp.einsum(
-            "rd,jdf->jrf", features, ups[:, own], preferred_element_type=jnp.float32
-        )
-        hidden = (jax.nn.silu(gated) * upward).astype(jnp.bfloat16)
-        result = jnp.einsum(
-            "jrf,jfd->rd", hidden, downs[:, own], preferred_element_type=jnp.float32
-        )
-        term = result * share
-        total = term if total is None else total + term
-    weighted = lax.psum_scatter(
-        total.astype(jnp.bfloat16), "sp", scatter_dimension=0, tiled=True
-    )
-    return (stream + weighted.astype(jnp.float32)).astype(jnp.bfloat16)
+        cost_estimate=pl.CostEstimate(
+            flops=8_000_000_000, bytes_accessed=20 * length * width, transcendentals=0
+        ),
+        name="experts",
+    )(features, stream, all_shares, gate, up, down, gates, ups, downs)
 
 
 def solution(mesh):

time: 269 us -> 182 us (0.68)
  waiting for transfers between devices: 149 us -> 0 us
  Pallas kernels: 65.2 us -> 159 us
  local copies, waits for them, and re-layouts: 1.01 us -> 22.1 us
  matrix products: 15.5 us -> 0 us
  starting transfers between devices: 13.8 us -> 0 us
  between operations: 13.7 us -> 0.07 us
  other arithmetic: 9.69 us -> 0.71 us
    pallas_call x4 -> x3, Pallas kernels: 65.2 us -> 159 us  [the longest x1 75.5 us: local(): pl.pallas_call(functools.partial(expert_kernel, PIECES, LAG), in_specs=[i...]
    reduce_scatter x2 -> x0, waiting for transfers between devices: 75.8 us -> none  [the longest x1 42.6 us: local(): lax.psum_scatter(total.astype(jnp.bfloat16), 'sp', scatter_dimension=0, t...]
    all_gather x4 -> x0, waiting for transfers between devices: 62.5 us -> none  [the longest x1 47.7 us: local(): lax.all_gather(jnp.concatenate([ffn_in, extra], axis=1), 'sp', axis=0, ti...]
    unnamed x21 -> x38, local copies, waits for them, and re-layouts: 0.88 us -> 22 us
    dot_general x4 -> x0, matrix products: 15.5 us -> none  [the longest x1 5.38 us: local(): jnp.einsum('rd,jdf->jrf', features, gates[:, own], preferred_element_type...]
    ppermute x3 -> x0, starting transfers between devices: 13.4 us -> none  [mixer(): got = lax.ppermute(sent, 'sp', [(i, i + 1) for i in range(axis_size - 1)])]
    ppermute x3 -> x0, waiting for transfers between devices: 8.65 us -> none  [mixer(): got = lax.ppermute(sent, 'sp', [(i, i + 1) for i in range(axis_size - 1)])]
    convert_element_type x4 -> x0, other arithmetic: 4.27 us -> none  [the longest x1 2.08 us: local(): return (stream + weighted.astype(jnp.float32)).astype(jnp.bfloat16)]
  transfers between devices with their start and end apart: 9 -> 0, of which waited for: 7 -> 0; matrix products, arithmetic and copies ran while one was open for 3% -> 0% of each run, Pallas kernels for 24% -> 0%
where the time goes in v1:
time: 182 us
  Pallas kernels  159 us (87%)
  local copies, waits for them, and re-layouts  22.1 us (12%)
    pallas_call x1, Pallas kernels, local(): pl.pallas_call(functools.partial(expert_kernel, PIECES, LAG), in_specs=[i...  75.5 us
    pallas_call x1, Pallas kernels, local(): pl.pallas_call(functools.partial(chunk_kernel, head_width), grid=(length...  60.8 us
    pallas_call x1, Pallas kernels, local(): pl.pallas_call(functools.partial(middle_kernel, head_width), in_specs=[in...  22.4 us
    unnamed x38, local copies, waits for them, and re-layouts  22 us

profile of v1, /device:TPU:0, one launch (start us, length us, event | category | flops | bytes accessed | tf_op | source)
XLA Modules:
  0.0 181.6 jit_solution(8391010681555614339)
XLA Ops:
  0.0 0.7 select_reduce_fusion
  0.7 0.1 copy.23
  0.8 0.8 copy.24.offset_ref
  1.7 0.0 copy-start
  1.7 1.2 copy-done
  2.9 0.0 copy-start.1
  2.9 1.2 copy-done.1
  4.1 0.0 copy-start.2
  4.1 1.2 copy-done.2
  5.4 0.0 copy-start.3
  5.4 1.0 copy-done.3
  6.4 0.0 copy-start.4
  6.4 1.0 copy-done.4
  7.4 0.0 copy-start.5
  7.5 1.0 copy-done.5
  8.5 0.0 copy-start.6
  8.5 1.0 copy-done.6
  9.5 0.0 copy-start.7
  9.5 1.0 copy-done.7
  10.6 0.0 copy-start.8
  10.6 0.7 copy-done.8
  11.3 0.0 copy-start.9
  11.3 0.7 copy-done.9
  11.9 60.8 %chunks.1 = (f32[512,512]{1,0:T(8,128)S(1)}, f32[512,512]{1,0:T(8,128)S(1)}, f32[64,512]{1,0:T(8,128)S(1)}, f32[64,512]{1,0:T(8,128)S(1)}, f32[4,128,128]{2,1,0:...) custom-call(bf16[512,512]{1,0:T(8,128)(2,1)S(1)} %copy-done.5, ...), custom_call_target="tpu_custom_call" | custom-call | flops 30000001024 | bytes 2097152 | tf_op jit(solution)/shard_map/chunks/pallas_call | solution.py:856
  72.8 0.0 copy-start.10
  72.8 1.6 copy-done.10
  74.4 0.0 copy-start.11
  74.4 1.7 copy-done.11
  76.1 0.0 copy-start.12
  76.1 1.7 copy-done.12
  77.8 0.0 copy-start.13
  77.8 1.0 copy-done.13
  78.8 0.0 copy-start.14
  78.8 1.0 copy-done.14
  79.8 0.0 copy-start.15
  79.8 0.7 copy-done.15
  80.5 0.0 copy-start.16
  80.5 0.7 copy-done.16
  81.1 0.0 copy-start.17
  81.1 0.6 copy-done.17
  81.8 22.4 %middle.1 = (f32[128,2048]{1,0:T(8,128)}, bf16[128,2048]{1,0:T(8,128)(2,1)}) custom-call(f32[512,512]{1,0:T(8,128)} %copy-done.13, f32[512,512]{1,0:T(8,128)} %copy-done.14, f32[64,512]{1,0:T(8,128)} %copy-done.16, f32[64,512]{1,0:T(8,128)} %copy-done.17, bf16[512,512]{1,0:T(8,128)(2,1)} %recept_ref.3, bf16[512,512]{1,0:T(8,128)(2,1)} %key_ref.3, ...), custom_call_target="tpu_custom_call" | custom-call | flops 8000000000 | bytes 5242880 | tf_op jit(solution)/shard_map/middle/pallas_call | solution.py:904
  104.2 75.5 %experts.1 = bf16[128,2048]{1,0:T(8,128)(2,1)} custom-call(bf16[128,2048]{1,0:T(8,128)(2,1)} %get-tuple-element.19.features_ref, f32[128,2048]{1,0:T(8,128)} %get-tuple-element.20.stream_ref, f32[4,128,128]{2,1,0:T(8,128)} %copy-done.15, bf16[2048,256]{1,0:T(8,128)(2,1)} %bitcast.8, bf16[2048,256]{1,0:T(8,128)(2,1)} %bitcast.10, bf16[256,2048]{1,0:T(8,128)(2,1)} %bitcast.12, ...), custom_call_target="tpu_custom_call" | custom-call | flops 8000000000 | bytes 5242880 | tf_op jit(solution)/shard_map/experts/pallas_call | solution.py:951
  179.8 1.9 %copy.26 = bf16[128,2048]{1,0:T(8,128)(2,1)} copy(bf16[128,2048]{1,0:T(8,128)(2,1)} %experts.1) | data formatting | bytes 1048576
  (1 shorter events, 0.0 us)
Async XLA Ops:
  1.7 1.2 copy-start
  2.9 1.2 copy-start.1
  4.1 1.2 copy-start.2
  5.4 1.0 copy-start.3
  6.4 1.0 copy-start.4
  7.4 1.0 copy-start.5
  8.5 1.0 copy-start.6
  9.5 1.0 copy-start.7
  10.6 0.7 copy-start.8
  11.3 0.7 copy-start.9
  72.8 1.7 copy-start.10
  74.4 1.7 copy-start.11
  76.1 1.7 copy-start.12
  77.8 1.0 copy-start.13
  78.8 1.0 copy-start.14
  79.8 0.7 copy-start.15
  80.5 0.7 copy-start.16
  81.1 0.6 copy-start.17

commit v2 on v0

v2 whole, which is shorter than its diff:
```python
import functools
import types
import typing

import jax
import jax.numpy as jnp
from jax import lax
from jax.experimental import pallas as pl
from jax.experimental.pallas import tpu as pltpu
from jax.sharding import PartitionSpec as P

SPAN = 64
LANES = 256
GROUP_EPS = 0.00064
NORM_EPS = 1e-06
NN = (((1,), (0,)), ((), ()))
NT = (((1,), (1,)), ((), ()))
MESH = pl.DeviceIdType.MESH
VMEM_LIMIT = 60 * 1024 * 1024


def peer(**coords):
    return tuple(coords.get(name, lax.axis_index(name)) for name in ("grp", "sp", "tp"))


def tp_peers():
    place = lax.axis_index("tp")
    chip, core = place // 2, place % 2
    return 2 * chip + 1 - core, 2 * (1 - chip) + core, 2 * (1 - chip) + 1 - core


def remote(src, dst, send_sem, recv_sem, device):
    return pltpu.make_async_remote_copy(
        src_ref=src,
        dst_ref=dst,
        send_sem=send_sem,
        recv_sem=recv_sem,
        device_id=device,
        device_id_type=MESH,
    )


def greet(barrier, device):
    pl.semaphore_signal(barrier, inc=1, device_id=device, device_id_type=MESH)


def halves(x):
    high = x.astype(jnp.bfloat16)
    return high, (x - high.astype(jnp.float32)).astype(jnp.bfloat16)


def product(left, right, dims):
    def dot(a, b):
        return lax.dot_general(a, b, dims, preferred_element_type=jnp.float32)

    return dot(left[0], right[0]) + (dot(left[1], right[0]) + dot(left[0], right[1]))


def block_mask(head_width):
    rows = lax.broadcasted_iota(jnp.int32, (LANES, LANES), 0) // head_width
    lanes = lax.broadcasted_iota(jnp.int32, (LANES, LANES), 1) // head_width
    return jnp.where(rows == lanes, 1.0, 0.0)


def spread_blocks(x, mask):
    copies = LANES // x.shape[0]
    return tuple(jnp.concatenate([part] * copies, axis=0) * mask for part in halves(x))


def head_sum(x, mask):
    high, low = halves(x)
    return lax.dot_general(
        high, mask, NN, preferred_element_type=jnp.float32
    ) + lax.dot_general(low, mask, NN, preferred_element_type=jnp.float32)


PORTIONS = ((0, 0, 4), (0, 4, 4), (1, 0, 4), (1, 4, 4), (2, 0, 4), (2, 4, 2), (2, 6, 2))
LATE = len(PORTIONS) - 1


class Gather:
    def __init__(self, own, full, sems):
        self.own, self.full = own, full
        (
            self.core_send,
            self.core_recv,
            self.chip_send,
            self.chip_recv,
            self.swap_send,
            self.swap_recv,
            self.pass_send,
            self.pass_recv,
            self.load,
        ) = sems
        near, far, _ = tp_peers()
        self.group = lax.axis_index("grp")
        self.near, self.far = peer(tp=near), peer(tp=far)
        self.twin = peer(grp=1 - self.group)

    def portion(self, refs, index, which, slot=None):
        k, first, size = PORTIONS[index]
        ref = refs[k]
        rows = ref.shape[-2] // 2
        unit = rows // 8
        start = pl.multiple_of(which * rows + first * unit, unit)
        at = pl.ds(start, size * unit)
        return ref.at[at] if slot is None else ref.at[slot, at]

    def core_copy(self, k):
        return remote(
            self.own[k], self.full[k].at[1], self.core_send.at[k], self.core_recv.at[k], self.near
        )

    def chip_copy(self, index):
        return remote(
            self.portion(self.own, index, self.group),
            self.portion(self.full, index, self.group, 2),
            self.chip_send.at[index],
            self.chip_recv.at[index],
            self.far,
        )

    def swap_copy(self, index, which):
        piece = self.portion(self.full, index, which, 2)
        return remote(
            piece, piece, self.swap_send.at[index], self.swap_recv.at[index], self.twin
        )

    def pass_copy(self, index, swapped):
        which = 1 - self.group if swapped else self.group
        slot = 2 * index + swapped
        return remote(
            self.portion(self.full, index, which, 2),
            self.portion(self.full, index, which, 3),
            self.pass_send.at[slot],
            self.pass_recv.at[slot],
            self.near,
        )

    def load_copy(self, k):
        return pltpu.make_async_copy(self.own[k], self.full[k].at[0], self.load.at[k])

    def begin(self):
        for index in range(LATE):
            self.chip_copy(index).start()
        for k in range(3):
            self.core_copy(k).start()
            self.load_copy(k).start()

    def begin_late(self):
        self.chip_copy(LATE).start()

    def arrive_chip(self, index):
        self.chip_copy(index).wait_recv()
        self.swap_copy(index, self.group).start()
        self.pass_copy(index, 0).start()

    def arrive_swap(self, index):
        self.swap_copy(index, 1 - self.group).wait_recv()
        self.pass_copy(index, 1).start()

    def arrive_rest(self):
        self.arrive_swap(LATE)
        for k in range(3):
            self.load_copy(k).wait()
            self.core_copy(k).wait_recv()
        for index in range(len(PORTIONS)):
            for swapped in range(2):
                self.pass_copy(index, swapped).wait_recv()

    def drain(self):
        for k in range(3):
            self.core_copy(k).wait_send()
        for index in range(len(PORTIONS)):
            self.chip_copy(index).wait_send()
            self.swap_copy(index, self.group).wait_send()
            for swapped in range(2):
                self.pass_copy(index, swapped).wait_send()


class Spread:
    def __init__(self, own, full, send, recv):
        self.own, self.full, self.send, self.recv = own, full, send, recv
        self.count = lax.axis_size("sp")
        self.place = lax.axis_index("sp")

    def greet(self, barrier):
        def one(ahead, carry):
            greet(barrier, peer(sp=(self.place + ahead) % self.count))
            return carry

        lax.fori_loop(1, self.count, one, 0)
        return self.count - 1

    def copy(self, ahead):
        return remote(
            self.own,
            self.full.at[self.place],
            self.send.at[ahead - 1],
            self.recv.at[self.place],
            peer(sp=(self.place + ahead) % self.count),
        )

    def arrival(self, ahead):
        source = (self.place + self.count - ahead) % self.count
        return remote(
            self.own,
            self.full.at[source],
            self.send.at[ahead - 1],
            self.recv.at[source],
            peer(sp=source),
        )

    def begin(self):
        self.full[self.place] = self.own[...]

        def one(ahead, carry):
            self.copy(ahead).start()
            return carry

        lax.fori_loop(1, self.count, one, 0)

    def end(self):
        def one(ahead, carry):
            self.copy(ahead).wait_send()
            self.arrival(ahead).wait_recv()
            return carry

        lax.fori_loop(1, self.count, one, 0)


def single(left, right, dims=NN):
    return lax.dot_general(
        left.astype(jnp.bfloat16),
        right.astype(jnp.bfloat16),
        dims,
        preferred_element_type=jnp.float32,
    )


def chunk_cells(head_width, refs, cells, offsets):
    recept_ref, key_ref, value_ref, decay_ref, rate_ref, decay_bias, rate_bias = refs
    span = head_width
    per_group = LANES // head_width
    wide_mask = block_mask(head_width)
    mask = wide_mask.astype(jnp.bfloat16)
    times = lax.broadcasted_iota(jnp.int32, (span, LANES), 0)
    lanes = lax.broadcasted_iota(jnp.int32, (span, LANES), 1)
    earlier = lanes % head_width
    strict = times > earlier
    within = times >= earlier
    eye = jnp.where(times == earlier, 1.0, 0.0)
    tri_rows = lax.broadcasted_iota(jnp.int32, (span, 3 * span), 0)
    tri_lanes = lax.broadcasted_iota(jnp.int32, (span, 3 * span), 1) % span
    tri = jnp.where(tri_rows >= tri_lanes, 1.0, 0.0).astype(jnp.bfloat16)

    def spread(x):
        return jnp.concatenate([x.astype(jnp.bfloat16)] * per_group, axis=0) * mask

    def each(step, *lists):
        return [step(*values) for values in zip(*lists)]

    def load(ref):
        return [ref[rows, cols].astype(jnp.float32) for rows, cols in cells]

    recept, key, value = load(recept_ref), load(key_ref), load(value_ref)

    def decays(cell, extra, by_head):
        cols = cell[1]
        offset = jnp.zeros((span, LANES), jnp.float32)
        for head in range(per_group):
            column = cols.start // head_width + head
            offset = jnp.where(
                lanes // head_width == head, by_head[:, column : column + 1], offset
            )
        return offset - 0.6065306597126334 / (1.0 + jnp.exp(-(decay_bias[:, cols] + extra)))

    decay = each(decays, cells, load(decay_ref), offsets)
    rate = each(
        lambda cell, extra: 1.0 / (1.0 + jnp.exp(-(rate_bias[:, cell[1]] + extra))),
        cells,
        load(rate_ref),
    )
    norm = each(lambda k: single(k * k, mask), key)
    unit = each(lambda k, n: k * lax.rsqrt(n + NORM_EPS), key, norm)

    def cumulative(d):
        one, rest = halves(d)
        third = (d - one.astype(jnp.float32) - rest.astype(jnp.float32)).astype(jnp.bfloat16)
        return single(tri, jnp.concatenate([third, rest, one], axis=0))

    cumul = each(cumulative, decay)
    middle = [c[span // 2 : span // 2 + 1] for c in cumul]
    last = [c[span - 1 : span] for c in cumul]
    center = each(lambda c, m: c - m, cumul, middle)
    grow = each(lambda c: jnp.exp(-c), center)
    remove = each(lambda u, c, d: -u * jnp.exp(c - d), unit, center, decay)
    reads = each(lambda r, c: r * jnp.exp(c), recept, center)
    write = each(lambda u, r, g: u * r * g, unit, rate, grow)
    keys = each(lambda k, g: k * g, key, grow)
    left = each(
        lambda a, b: jnp.concatenate([a, b], axis=0).astype(jnp.bfloat16), remove, reads
    )
    by_write = each(lambda a, b: single(a, spread(b), NT), left, write)
    by_key = each(lambda a, b: single(a, spread(b), NT), left, keys)
    remove_write = [jnp.where(strict, x[:span], 0.0) for x in by_write]
    read_write = [jnp.where(within, x[span:], 0.0).astype(jnp.bfloat16) for x in by_write]
    key_rows = [
        jnp.concatenate(
            [jnp.where(strict, x[:span], 0.0), jnp.where(within, x[span:], 0.0)], axis=0
        )
        for x in by_key
    ]
    from_value = each(
        lambda a, b: sum(single(part, spread(b)) for part in halves(a)), key_rows, value
    )
    inverse = [eye + jnp.where(times // 2 == earlier // 2, x, 0.0) for x in remove_write]
    size = 2
    while size < span:
        joint = (times // (2 * size) == earlier // (2 * size)) & (
            times // size != earlier // size
        )
        step = each(
            lambda a, b: single(a, spread(jnp.where(joint, b, 0.0))), inverse, remove_write
        )
        inverse = each(lambda a, b: b + single(a, spread(b)), step, inverse)
        size *= 2
    start = [jnp.exp(m) for m in middle]
    inverse = [halves(x) for x in inverse]
    inv_remove = each(
        lambda a, b, c: product(a, spread_blocks(b, mask), NN) * c, inverse, remove, start
    )
    inv_value = each(
        lambda a, b: product(a, spread_blocks(b[:span], mask), NN), inverse, from_value
    )
    read_map = each(
        lambda a, b, c, d: a * b + single(c, spread(d)), reads, start, read_write, inv_remove
    )
    read_own = each(
        lambda a, b, c: a[span:] + single(b, spread(c)), from_value, read_write, inv_value
    )
    tail = each(lambda a, b: jnp.exp(a - b), last, middle)
    write_end = each(lambda a, b: a * b, write, tail)
    key_end = each(lambda a, b: a * b, keys, tail)
    low = each(lambda a, b: single(a.T, b) * wide_mask, inv_remove, write_end)

    def gained(a, b, c, d):
        full = (
            single(jnp.concatenate([a, b], axis=0).T, jnp.concatenate([c, d], axis=0)) * wide_mask
        )
        return sum(full[h * head_width : (h + 1) * head_width] for h in range(per_group))

    added = each(gained, inv_value, value, write_end, key_end)
    kept = [jnp.exp(x) for x in last]
    return read_map, read_own, low, kept, added, spread


def mixed_rows(head_width, rows, state, refs, mask):
    map_ref, own_ref, recept_ref, key_ref, value_ref, gate_ref, gain_ref, self_ref = refs
    groups = [slice(g * LANES, (g + 1) * LANES) for g in range(map_ref.shape[1] // LANES)]
    copies = LANES // head_width

    def spread(x):
        return jnp.concatenate([x.astype(jnp.bfloat16)] * copies, axis=0) * mask

    read = [
        own_ref[rows, cols] + single(map_ref[rows, cols], spread(state[g]), NT)
        for g, cols in enumerate(groups)
    ]
    own = [
        head_sum(
            recept_ref[rows, cols].astype(jnp.float32)
            * key_ref[rows, cols].astype(jnp.float32)
            * self_ref[:, cols],
            mask,
        )
        * value_ref[rows, cols].astype(jnp.float32)
        for cols in groups
    ]
    off = [x - head_sum(x, mask) * (1.0 / head_width) for x in read]
    width = [single(x * x, mask) * (1.0 / head_width) for x in off]
    return [
        (
            (off[g] * lax.rsqrt(width[g] + GROUP_EPS) * gain_ref[:, cols] + own[g])
            * gate_ref[rows, cols].astype(jnp.float32)
        ).astype(jnp.bfloat16)
        for g, cols in enumerate(groups)
    ]


class Inputs(typing.NamedTuple):
    recept: typing.Any
    key: typing.Any
    value: typing.Any
    decay: typing.Any
    rate: typing.Any
    offset: typing.Any
    decay_bias: typing.Any
    rate_bias: typing.Any
    gain: typing.Any
    self_weight: typing.Any
    norm_gain: typing.Any
    share: typing.Any
    output_gate: typing.Any
    out_weight: typing.Any
    residual: typing.Any
    gate: typing.Any
    up: typing.Any
    down: typing.Any


class InnerSems(typing.NamedTuple):
    load: typing.Any
    state_send: typing.Any
    state_recv: typing.Any
    sum_core_send: typing.Any
    sum_core_recv: typing.Any
    sum_chip_send: typing.Any
    sum_chip_recv: typing.Any
    core_send: typing.Any
    core_recv: typing.Any
    chip_send: typing.Any
    chip_recv: typing.Any
    swap_send: typing.Any
    swap_recv: typing.Any
    pass_send: typing.Any
    pass_recv: typing.Any
    weight_load: typing.Any
    share_send: typing.Any
    share_recv: typing.Any


class Flows(typing.NamedTuple):
    blocks: typing.Any
    result: typing.Any
    from_right: typing.Any
    from_left: typing.Any
    to_left: typing.Any
    to_right: typing.Any


class FlowSems(typing.NamedTuple):
    gather_send: typing.Any
    gather_recv: typing.Any
    flow_send: typing.Any
    flow_recv: typing.Any


def layer_kernel(names, head_width, pieces, lag, *all_refs):
    ref = types.SimpleNamespace(**dict(zip(names, all_refs, strict=True)))
    with_experts = hasattr(ref, "out")
    place, count = lax.axis_index("sp"), lax.axis_size("sp")
    near, far, cross = tp_peers()
    mine = lax.axis_index("tp")
    ahead, behind = peer(sp=(place + 1) % count), peer(sp=(place + count - 1) % count)
    has_left, has_right = place > 0, place < count - 1
    length, width = ref.recept_all.shape
    groups = [slice(g * LANES, (g + 1) * LANES) for g in range(width // LANES)]
    rows = ref.residual.shape[0]
    size = rows // pieces
    mask = block_mask(head_width).astype(jnp.bfloat16)

    weights = Gather(
        (ref.gate, ref.up, ref.down),
        (ref.gates, ref.ups, ref.downs),
        tuple(getattr(ref, name) for name in InnerSems._fields[7:16]),
    )
    shares = Spread(ref.share, ref.shares, ref.share_send, ref.share_recv)
    barrier = pltpu.get_barrier_semaphore()
    for device in (weights.near, weights.far, weights.twin):
        greet(barrier, device)
    pl.semaphore_wait(barrier, 3 + shares.greet(barrier))
    weights.begin()
    shares.begin()
    loads = [
        pltpu.make_async_copy(source, held, ref.load.at[k])
        for k, (source, held) in enumerate(
            (
                (ref.recept, ref.recept_all),
                (ref.key, ref.key_all),
                (ref.value, ref.value_all),
                (ref.decay, ref.decay_all),
                (ref.rate, ref.rate_all),
                (ref.output_gate, ref.output_gate_all),
                (ref.out_weight, ref.out_weight_all),
                (ref.residual, ref.residual_all),
            )
        )
    ]
    for load in loads:
        load.start()
    for load in loads[:5]:
        load.wait()

    full_lanes = lax.broadcasted_iota(jnp.int32, ref.transit.shape, 1) % head_width
    full_rows = lax.broadcasted_iota(jnp.int32, ref.transit.shape, 0)
    ref.transit[...] = jnp.where(full_lanes == full_rows, 1.0, 0.0)
    ref.added[...] = jnp.zeros_like(ref.added)
    chunk_refs = (ref.recept_all, ref.key_all, ref.value_all, ref.decay_all, ref.rate_all, ref.decay_bias, ref.rate_bias)
    per_step = 2

    def chunk_step(step, carry):
        cells, offsets = [], []
        span = per_step * head_width
        by_head = ref.offset[:, pl.ds(pl.multiple_of(step * span, span), span)].T
        for chunk in range(per_step):
            own_offset = by_head[chunk * head_width : (chunk + 1) * head_width]
            offsets += [own_offset] * len(groups)
            first = pl.multiple_of((step * per_step + chunk) * head_width, head_width)
            cells += [(pl.ds(first, head_width), cols) for cols in groups]
        read_map, read_own, low, kept, added, spread = chunk_cells(
            head_width, chunk_refs, cells, offsets
        )
        for k, at in enumerate(cells):
            cols = at[1]
            held_transit, held_added = ref.transit[:, cols], ref.added[:, cols]
            ref.map[at] = single(read_map[k], spread(held_transit), NT).astype(jnp.bfloat16)
            ref.own[at] = read_own[k] + single(read_map[k], spread(held_added), NT)
            held = jnp.concatenate([held_transit, held_added], axis=0)
            moved = held * kept[k] + single(held, low[k])
            ref.transit[:, cols] = moved[:head_width]
            ref.added[:, cols] = moved[head_width:] + added[k]

        for index in range(2):
            pl.when(step == index + 1)(functools.partial(weights.arrive_chip, index))

        return carry

    lax.fori_loop(0, length // (per_step * head_width), chunk_step, 0)

    state_ref, onward_ref = ref.state, ref.onward

    def state_copy(group):
        return remote(
            onward_ref.at[group],
            state_ref.at[group],
            ref.state_send.at[group],
            ref.state_recv.at[group],
            ahead,
        )

    @pl.when(place == 0)
    def _():
        for group, cols in enumerate(groups):
            state_ref[group] = jnp.zeros_like(state_ref[group])
            onward_ref[group] = ref.added[:, cols]
            state_copy(group).start()

    weights.arrive_chip(2)

    @pl.when(has_left)
    def _():
        for group, cols in enumerate(groups):
            state_copy(group).wait_recv()

            @pl.when(has_right)
            def _(group=group, cols=cols):
                onward_ref[group] = ref.added[:, cols] + product(
                    halves(state_ref[group]), spread_blocks(ref.transit[:, cols], mask), NN
                )
                state_copy(group).start()

    weights.arrive_chip(3)
    weights.arrive_swap(0)
    weights.arrive_swap(1)
    for load in loads[5:]:
        load.wait()

    mixed_refs = (ref.map, ref.own, ref.recept_all, ref.key_all, ref.value_all, ref.output_gate_all, ref.gain, ref.self_weight)
    core_out, core_in = ref.core_out, ref.core_in
    chip_out, chip_in = ref.chip_out, ref.chip_in

    def partial(owner, part):
        at = pl.ds(pl.multiple_of(owner * rows + part * size, size), size)
        mixed = mixed_rows(head_width, at, state_ref, mixed_refs, mask)
        return single(jnp.concatenate(mixed, axis=1), ref.out_weight_all[...])

    def core_copy(which, part):
        slot = which * pieces + part
        return remote(
            core_out.at[slot],
            core_in.at[slot],
            ref.sum_core_send.at[slot],
            ref.sum_core_recv.at[slot],
            weights.near,
        )

    def chip_copy(part):
        return remote(
            chip_out.at[part],
            chip_in.at[part],
            ref.sum_chip_send.at[part],
            ref.sum_chip_recv.at[part],
            weights.far,
        )

    stream_ref, features_ref = ref.stream, ref.features
    for part in range(pieces):
        core_out[part] = partial(cross, part)
        core_copy(0, part).start()
        own = partial(far, part)
        core_copy(0, part).wait_recv()
        chip_out[part] = (own + core_in[part]).astype(jnp.bfloat16)
        chip_copy(part).start()
        if part == 0:
            weights.begin_late()
    weights.arrive_chip(4)
    weights.arrive_chip(5)

    def sum_own(part):
        at = slice(part * size, (part + 1) * size)
        core_out[pieces + part] = partial(near, part)
        core_copy(1, part).start()
        own = partial(mine, part)
        core_copy(1, part).wait_recv()
        stream_ref[at] = (
            ref.residual_all[at].astype(jnp.float32) + own + core_in[pieces + part]
        )

    def pass_late():
        weights.arrive_swap(4)
        weights.arrive_swap(5)

    def finish_stream(part):
        sum_own(part)
        if part == pieces - 1:
            weights.arrive_chip(LATE)
            weights.arrive_swap(2)
            weights.arrive_swap(3)
        at = slice(part * size, (part + 1) * size)
        chip_copy(part).wait_recv()
        stream = stream_ref[at] + chip_in[part].astype(jnp.float32)
        stream_ref[at] = stream
        features_ref[at] = (
            stream
            * lax.rsqrt(jnp.mean(stream * stream, axis=-1, keepdims=True) + NORM_EPS)
            * ref.norm_gain[...]
        ).astype(jnp.bfloat16)

    def drain_first():
        @pl.when(has_right)
        def _():
            for group in range(len(groups)):
                state_copy(group).wait_send()

        for part in range(pieces):
            core_copy(0, part).wait_send()
            core_copy(1, part).wait_send()
            chip_copy(part).wait_send()
        weights.drain()

    if not with_experts:
        for part in range(pieces):
            finish_stream(part)
        pass_late()
        weights.arrive_rest()
        shares.end()
        drain_first()
        return

    blocks, result, from_right, from_left, to_left, to_right = (getattr(ref, name) for name in Flows._fields)

    def gather_copy(source, block, piece, part, way):
        return remote(
            source,
            blocks.at[block, piece, part],
            ref.gather_send.at[way, block, piece, part],
            ref.gather_recv.at[block, piece, part],
            ahead if way else behind,
        )

    def sum_copy(block, piece, part, way):
        out, into = (to_right, from_left) if way else (to_left, from_right)
        return remote(
            out.at[block, piece, part],
            into.at[block, piece, part],
            ref.flow_send.at[way, block, piece, part],
            ref.flow_recv.at[way, block, piece, part],
            ahead if way else behind,
        )

    parts = blocks.shape[2]
    fine = blocks.shape[3]

    def send_own(piece, way):
        for part in range(parts):
            own_features = features_ref.at[pl.ds(piece * size + part * fine, fine)]
            gather_copy(own_features, place, piece, part, way).start()

    finish_stream(0)
    pl.when(has_left)(lambda: send_own(0, 0))
    pl.when(has_right)(lambda: send_own(0, 1))
    finish_stream(1)
    pl.when(has_left & (place == count - 1))(lambda: send_own(1, 0))
    pl.when(has_right & (place == 0))(lambda: send_own(1, 1))

    def apply(features, block, piece):
        total = None
        for j in range(ref.gates.shape[0]):
            gated = single(features, ref.gates[j])
            upward = single(features, ref.ups[j])
            term = single(jax.nn.silu(gated) * upward, ref.downs[j])
            total = term if total is None else total + term
        own = ref.shares[block, pl.ds(pl.multiple_of(piece * size, size), size)]
        lanes = lax.broadcasted_iota(jnp.int32, own.shape, 1)
        share = jnp.sum(jnp.where(lanes == place, own, 0.0), axis=1, keepdims=True)
        result[block, piece] = (total * share).reshape(parts, fine, total.shape[1])

    def slot(time, carry):
        arrivals = []
        for way, before in ((1, place), (0, count - 1 - place)):
            step = 1 if way else -1
            far = 0 if way else count - 1
            first = time < before
            block = jnp.where(first, place - step * (1 + time), far + step * (time - before))
            piece = jnp.where(first, 0, 1)
            arrivals.append((way, block, piece, time < 2 * before, time == 2 * before - 1))

        for way, block, piece, there, final in arrivals:
            onward = has_right if way else has_left

            @pl.when(there)
            def _(way=way, block=block, piece=piece, onward=onward, final=final):
                for part in range(parts):
                    landed = blocks.at[block, piece, part]
                    gather_copy(landed, block, piece, part, way).wait_recv()
                    pl.when(onward)(
                        lambda: gather_copy(landed, block, piece, part, way).start()
                    )
                pl.when(onward & final)(lambda: send_own(1, way))

        @pl.when(time == 0)
        def _():
            pass_late()
            weights.arrive_rest()
            shares.end()

        own = time - 2 * (count - 1)

        @pl.when((own >= 0) & (own < pieces))
        def _():
            at = pl.ds(pl.multiple_of(own * size, size), size)
            apply(features_ref[at], place, own)

        for way, block, piece, there, final in arrivals:

            @pl.when(there)
            def _(block=block, piece=piece):
                features = blocks[block, piece]
                apply(features.reshape(size, features.shape[2]), block, piece)

        for way, hops, more, into, out in (
            (0, count - 1 - place, has_right, from_right, to_left),
            (1, place, has_left, from_left, to_right),
        ):
            turn = time - lag * hops
            first = turn < count - 1
            offset = jnp.where(first, count - 2 - turn, turn - (count - 1))
            block = count - 1 - offset if way else offset
            piece = jnp.where(first, 0, 1)
            passed = block - place if way else place - block
            valid = (turn >= 0) & (turn < 2 * (count - 1)) & (passed >= 0)

            for part in range(parts):

                @pl.when(valid & more)
                def _(way=way, block=block, piece=piece, part=part, into=into):
                    sum_copy(block, piece, part, way).wait_recv()

                @pl.when(valid & more & (passed > 0))
                def _(block=block, piece=piece, part=part, into=into, out=out):
                    total = result[block, piece, part] + into[block, piece, part].astype(
                        jnp.float32
                    )
                    out[block, piece, part] = total.astype(jnp.bfloat16)

                @pl.when(valid & jnp.logical_not(more))
                def _(block=block, piece=piece, part=part, out=out):
                    out[block, piece, part] = result[block, piece, part].astype(jnp.bfloat16)

                @pl.when(valid & (passed > 0))
                def _(way=way, block=block, piece=piece, part=part):
                    sum_copy(block, piece, part, way).start()

        return carry

    lax.fori_loop(0, (2 + lag) * (count - 1), slot, 0)
    for piece in range(pieces):
        at = slice(piece * size, (piece + 1) * size)
        shape = (size, stream_ref.shape[1])
        stream_ref[at] = stream_ref[at] + result[place, piece].reshape(shape)
        for there, into in ((has_right, from_right), (has_left, from_left)):

            @pl.when(there)
            def _(at=at, into=into, piece=piece):
                stream_ref[at] = stream_ref[at] + into[place, piece].reshape(shape).astype(
                    jnp.float32
                )

        ref.out[at] = stream_ref[at].astype(jnp.bfloat16)

    def drain(block, carry):
        for piece in range(pieces):
            for part in range(parts):
                landed = blocks.at[block, piece, part]
                for way, gathers, sums in (
                    (0, has_left & (block >= place), has_left & (block < place)),
                    (1, has_right & (block <= place), has_right & (block > place)),
                ):
                    pl.when(gathers)(
                        lambda: gather_copy(landed, block, piece, part, way).wait_send()
                    )
                    pl.when(sums)(lambda: sum_copy(block, piece, part, way).wait_send())
        return carry

    lax.fori_loop(0, count, drain, 0)
    drain_first()


def shares_of(routed_expert_index, routed_expert_weight, experts):
    ids = jnp.arange(experts + -experts % 128, dtype=jnp.int32)
    return jnp.sum(
        jnp.where(
            routed_expert_index[:, :, None] == ids, routed_expert_weight[:, :, None], 0.0
        ),
        axis=1,
    )


def experts_by_collectives(features, stream, shares, gates, ups, downs):
    features = lax.all_gather(features, "sp", axis=0, tiled=True)
    shares = shares.reshape(-1, shares.shape[-1])
    place = lax.axis_index("sp")
    lanes = jnp.arange(shares.shape[1], dtype=jnp.int32)
    share = jnp.sum(jnp.where(lanes[None, :] == place, shares, 0.0), axis=1, keepdims=True)
    depth = features.shape[1]

    def some_rows(operands):
        features, share = operands
        total = None
        for gate, up, down in zip(gates, ups, downs):
            for j in range(gate.shape[0]):
                gated = jnp.dot(features, gate[j], preferred_element_type=jnp.float32)
                upward = jnp.dot(features, up[j], preferred_element_type=jnp.float32)
                hidden = (jax.nn.silu(gated) * upward).astype(jnp.bfloat16)
                term = jnp.dot(hidden, down[j], preferred_element_type=jnp.float32)
                total = term if total is None else total + term
        return (total * share).astype(jnp.bfloat16)

    rows = stream.shape[0]
    total = lax.map(
        some_rows, (features.reshape(-1, rows, depth), share.reshape(-1, rows, 1))
    ).reshape(-1, depth)
    weighted = lax.psum_scatter(total, "sp", scatter_dimension=0, tiled=True)
    return (stream + weighted.astype(jnp.float32)).astype(jnp.bfloat16)


PIECES = 2
PARTS = 2
LAG = 1


def local(
    recept,
    key_input,
    value_input,
    output_gate_input,
    decay_input_part,
    correction_rate_input,
    head_decay_offset,
    decay_fixed_bias,
    correction_rate_bias,
    head_norm_gain,
    self_term_weight,
    output_weight_matrix,
    residual,
    feedforward_norm_gain,
    routed_expert_index,
    routed_expert_weight,
    gate_weight_experts,
    up_weight_experts,
    down_weight_experts,
):
    count = lax.axis_size("sp")
    experts = gate_weight_experts.shape[0] * count
    assert lax.axis_size("tp") == 4 and lax.axis_size("grp") == 2
    assert gate_weight_experts.shape[0] == 1
    length, width = recept.shape
    heads = head_decay_offset.shape[1]
    head_width = width // heads
    own_rows, depth = residual.shape
    shares = shares_of(routed_expert_index, routed_expert_weight, experts)
    gate, up, down = gate_weight_experts[0], up_weight_experts[0], down_weight_experts[0]
    groups = width // LANES
    half = own_rows // PIECES
    dma = pltpu.SemaphoreType.DMA
    single_bf, single_f32 = jnp.bfloat16, jnp.float32

    def like(x):
        return (x.shape, x.dtype)

    kept = dict(
        stream=((own_rows, depth), single_f32),
        features=((own_rows, depth), single_bf),
        shares=((count, *shares.shape), single_f32),
        gates=((4, *gate.shape), gate.dtype),
        ups=((4, *up.shape), up.dtype),
        downs=((4, *down.shape), down.dtype),
    )
    sums = ((2 * PIECES, half, depth), single_f32)
    chips = ((PIECES, half, depth), single_bf)
    states = ((groups, head_width, LANES), single_f32)
    inner = dict(
        recept_all=like(recept),
        key_all=like(key_input),
        value_all=like(value_input),
        decay_all=like(decay_input_part),
        rate_all=like(correction_rate_input),
        output_gate_all=like(output_gate_input),
        out_weight_all=like(output_weight_matrix),
        residual_all=like(residual),
        map=((length, width), single_bf),
        own=((length, width), single_f32),
        transit=((head_width, width), single_f32),
        added=((head_width, width), single_f32),
        state=states,
        onward=states,
        core_out=sums,
        core_in=sums,
        chip_out=chips,
        chip_in=chips,
    )
    sems = [(8,), (groups,), (groups,)] + [(2 * PIECES,)] * 2 + [(PIECES,)] * 2
    portions = len(PORTIONS)
    sems += [(3,)] * 2 + [(portions,)] * 4 + [(2 * portions,)] * 2 + [(3,), (count,), (count,)]
    inner_sems = dict(zip(InnerSems._fields, sems, strict=True))
    with_experts = count <= 4
    scratch, outs = dict(inner), dict(kept)
    if with_experts:
        flow = ((count, PIECES, PARTS, half // PARTS, depth), single_bf)
        scratch = kept | inner
        scratch |= {name: flow for name in Flows._fields} | dict(result=(flow[0], single_f32))
        outs = dict(out=((own_rows, depth), single_bf))
        both = (2, count, PIECES, PARTS)
        inner_sems |= dict(zip(FlowSems._fields, (both, both[1:], both, both), strict=True))
    names = [*Inputs._fields, *outs, *scratch, *inner_sems]
    anywhere = pl.BlockSpec(memory_space=pl.ANY)
    in_vmem = pl.BlockSpec(memory_space=pltpu.VMEM)
    results = pl.pallas_call(
        functools.partial(layer_kernel, names, head_width, PIECES, LAG),
        in_specs=[anywhere] * 5 + [in_vmem] * 7 + [anywhere] * 6,
        out_specs=[in_vmem] * len(outs),
        out_shape=[jax.ShapeDtypeStruct(*spec) for spec in outs.values()],
        scratch_shapes=[pltpu.VMEM(*spec) for spec in scratch.values()]
        + [dma(shape) for shape in inner_sems.values()],
        compiler_params=pltpu.CompilerParams(
            collective_id=0, has_side_effects=True, vmem_limit_bytes=VMEM_LIMIT
        ),
        cost_estimate=pl.CostEstimate(
            flops=30_000_000_000, bytes_accessed=40 * length * width, transcendentals=0
        ),
        name="layer",
    )(
        recept,
        key_input,
        value_input,
        decay_input_part,
        correction_rate_input,
        head_decay_offset.T,
        decay_fixed_bias[None],
        correction_rate_bias[None],
        head_norm_gain[None],
        self_term_weight[None],
        feedforward_norm_gain[None],
        shares,
        output_gate_input,
        output_weight_matrix,
        residual,
        gate,
        up,
        down,
    )
    if with_experts:
        return results[0]
    stream, features, all_shares, *full = results
    return experts_by_collectives(features, stream, all_shares, *((each,) for each in full))


def solution(mesh):
    return jax.shard_map(
        local,
        mesh=mesh,
        in_specs=(
            P(("grp", "sp"), "tp"),
            P(("grp", "sp"), "tp"),
            P(("grp", "sp"), "tp"),
            P(("grp", "sp"), "tp"),
            P(("grp", "sp"), "tp"),
            P(("grp", "sp"), "tp"),
            P(("grp", "sp"), "tp"),
            P("tp"),
            P("tp"),
            P("tp"),
            P("tp"),
            P("tp", None),
            P(("grp", "sp", "tp"), None),
            P(),
            P(("grp", "sp", "tp"), None),
            P(("grp", "sp", "tp"), None),
            P("sp", None, "tp"),
            P("sp", None, "tp"),
            P("sp", "tp", None),
        ),
        out_specs=P(("grp", "sp", "tp"), None),
        check_vma=False,
    )
```

time: 269 us -> 105 us (0.39)
  waiting for transfers between devices: 149 us -> 0 us
  Pallas kernels: 65.2 us -> 102 us
  matrix products: 15.5 us -> 0 us
  starting transfers between devices: 13.8 us -> 0 us
  between operations: 13.7 us -> 0.01 us
  other arithmetic: 9.69 us -> 1.46 us
    reduce_scatter x2 -> x0, waiting for transfers between devices: 75.8 us -> none  [the longest x1 42.6 us: local(): lax.psum_scatter(total.astype(jnp.bfloat16), 'sp', scatter_dimension=0, t...]
    all_gather x4 -> x0, waiting for transfers between devices: 62.5 us -> none  [the longest x1 47.7 us: local(): lax.all_gather(jnp.concatenate([ffn_in, extra], axis=1), 'sp', axis=0, ti...]
    pallas_call x4 -> x1, Pallas kernels: 65.2 us -> 102 us  [local(): pl.pallas_call(functools.partial(layer_kernel, names, head_width, PIECES,...]
    dot_general x4 -> x0, matrix products: 15.5 us -> none  [the longest x1 5.38 us: local(): jnp.einsum('rd,jdf->jrf', features, gates[:, own], preferred_element_type...]
    ppermute x3 -> x0, starting transfers between devices: 13.4 us -> none  [mixer(): got = lax.ppermute(sent, 'sp', [(i, i + 1) for i in range(axis_size - 1)])]
    ppermute x3 -> x0, waiting for transfers between devices: 8.65 us -> none  [mixer(): got = lax.ppermute(sent, 'sp', [(i, i + 1) for i in range(axis_size - 1)])]
    convert_element_type x4 -> x0, other arithmetic: 4.27 us -> none  [the longest x1 2.08 us: local(): return (stream + weighted.astype(jnp.float32)).astype(jnp.bfloat16)]
    select_n x3 -> x0, other arithmetic: 2.93 us -> none  [mixer(): state = jnp.where(place == lap + 1, got, state)]
  transfers between devices with their start and end apart: 9 -> 0, of which waited for: 7 -> 0; matrix products, arithmetic and copies ran while one was open for 3% -> 0% of each run, Pallas kernels for 24% -> 0%
where the time goes in v2:
time: 105 us
  Pallas kernels  102 us (97%)
  local copies, waits for them, and re-layouts  1.88 us (2%)
  other arithmetic  1.46 us (1%)
    pallas_call x1, Pallas kernels, local(): pl.pallas_call(functools.partial(layer_kernel, names, head_width, PIECES,...  102 us

profile of v2, /device:TPU:0, one launch (start us, length us, event | category | flops | bytes accessed | tf_op | source)
XLA Modules:
  0.0 105.1 jit_solution(6087762300020328752)
XLA Ops:
  0.0 1.5 %select_reduce_fusion.all_refs_11_ = f32[128,128]{1,0:T(8,128)} fusion(f32[128,2]{0,1:T(2,128)} %param.34, s32[128,2]{0,1:T(2,128)} %param.33), kind=kLoop, calls=%fused_computation | loop fusion | flops 81920 | bytes 67584 | tf_op jit(solution)/shard_map/reduce_sum | solution.py:822
  1.5 101.7 %layer.1 = bf16[128,2048]{1,0:T(8,128)(2,1)} custom-call(bf16[512,512]{1,0:T(8,128)(2,1)} %all_refs_0_.1, bf16[512,512]{1,0:T(8,128)(2,1)} %all_refs_1_.1, bf16[512,512]{1,0:T(8,128)(2,1)} %all_refs_2_.1, bf16[512,512]{1,0:T(8,128)(2,1)} %all_refs_3_.1, bf16[512,512]{1,0:T(8,128)(2,1)} %all_refs_4_.1, f32[8,512]{1,0:T(8,128)} %bitcast.12, ...), custom_call_target="tpu_custom_call" | custom-call | flops 30000001024 | bytes 10485760 | tf_op jit(solution)/shard_map/layer/pallas_call | solution.py:949
  103.2 1.9 %copy.23 = bf16[128,2048]{1,0:T(8,128)(2,1)} copy(bf16[128,2048]{1,0:T(8,128)(2,1)} %layer.1) | data formatting | bytes 1048576

commit v3 on v2

--- a/solution.py
+++ b/solution.py
@@ -326,13 +326,13 @@
         inverse = each(lambda a, b: b + single(a, spread(b)), step, inverse)
         size *= 2
     start = [jnp.exp(m) for m in middle]
-    inverse = [halves(x) for x in inverse]
-    inv_remove = each(
-        lambda a, b, c: product(a, spread_blocks(b, mask), NN) * c, inverse, remove, start
-    )
-    inv_value = each(
-        lambda a, b: product(a, spread_blocks(b[:span], mask), NN), inverse, from_value
-    )
+    inverse = [x.astype(jnp.bfloat16) for x in inverse]
+
+    def applied(a, b):
+        return sum(single(a, part) for part in spread_blocks(b, mask))
+
+    inv_remove = each(lambda a, b, c: applied(a, b) * c, inverse, remove, start)
+    inv_value = each(lambda a, b: applied(a, b[:span]), inverse, from_value)
     read_map = each(
         lambda a, b, c, d: a * b + single(c, spread(d)), reads, start, read_write, inv_remove
     )
@@ -400,7 +400,8 @@
     gain: typing.Any
     self_weight: typing.Any
     norm_gain: typing.Any
-    share: typing.Any
+    route_index: typing.Any
+    route_weight: typing.Any
     output_gate: typing.Any
     out_weight: typing.Any
     residual: typing.Any
@@ -471,7 +472,6 @@
         greet(barrier, device)
     pl.semaphore_wait(barrier, 3 + shares.greet(barrier))
     weights.begin()
-    shares.begin()
     loads = [
         pltpu.make_async_copy(source, held, ref.load.at[k])
         for k, (source, held) in enumerate(
@@ -492,6 +492,14 @@
     for load in loads[:5]:
         load.wait()
 
+    named = ref.route_index[...].astype(jnp.float32).T
+    weight = ref.route_weight[...].T
+    ids = lax.broadcasted_iota(jnp.int32, ref.share.shape, 1).astype(jnp.float32)
+    ref.share[...] = sum(
+        jnp.where(named[:, k : k + 1] == ids, weight[:, k : k + 1], 0.0)
+        for k in range(named.shape[1])
+    )
+
     full_lanes = lax.broadcasted_iota(jnp.int32, ref.transit.shape, 1) % head_width
     full_rows = lax.broadcasted_iota(jnp.int32, ref.transit.shape, 0)
     ref.transit[...] = jnp.where(full_lanes == full_rows, 1.0, 0.0)
@@ -527,6 +535,8 @@
         return carry
 
     lax.fori_loop(0, length // (per_step * head_width), chunk_step, 0)
+
+    shares.begin()
 
     state_ref, onward_ref = ref.state, ref.onward
 
@@ -815,16 +825,6 @@
 
     lax.fori_loop(0, count, drain, 0)
     drain_first()
-
-
-def shares_of(routed_expert_index, routed_expert_weight, experts):
-    ids = jnp.arange(experts + -experts % 128, dtype=jnp.int32)
-    return jnp.sum(
-        jnp.where(
-            routed_expert_index[:, :, None] == ids, routed_expert_weight[:, :, None], 0.0
-        ),
-        axis=1,
-    )
 
 
 def experts_by_collectives(features, stream, shares, gates, ups, downs):
@@ -889,7 +889,7 @@
     heads = head_decay_offset.shape[1]
     head_width = width // heads
     own_rows, depth = residual.shape
-    shares = shares_of(routed_expert_index, routed_expert_weight, experts)
+    shares = jax.ShapeDtypeStruct((residual.shape[0], experts + -experts % 128), jnp.float32)
     gate, up, down = gate_weight_experts[0], up_weight_experts[0], down_weight_experts[0]
     groups = width // LANES
     half = own_rows // PIECES
@@ -919,6 +919,7 @@
         output_gate_all=like(output_gate_input),
         out_weight_all=like(output_weight_matrix),
         residual_all=like(residual),
+        share=like(shares),
         map=((length, width), single_bf),
         own=((length, width), single_f32),
         transit=((head_width, width), single_f32),
@@ -948,7 +949,7 @@
     in_vmem = pl.BlockSpec(memory_space=pltpu.VMEM)
     results = pl.pallas_call(
         functools.partial(layer_kernel, names, head_width, PIECES, LAG),
-        in_specs=[anywhere] * 5 + [in_vmem] * 7 + [anywhere] * 6,
+        in_specs=[anywhere] * 5 + [in_vmem] * 8 + [anywhere] * 6,
         out_specs=[in_vmem] * len(outs),
         out_shape=[jax.ShapeDtypeStruct(*spec) for spec in outs.values()],
         scratch_shapes=[pltpu.VMEM(*spec) for spec in scratch.values()]
@@ -972,7 +973,8 @@
         head_norm_gain[None],
         self_term_weight[None],
         feedforward_norm_gain[None],
-        shares,
+        routed_expert_index.T,
+        routed_expert_weight.T,
         output_gate_input,
         output_weight_matrix,
         residual,

time: 105 us -> 106 us (level)
  Pallas kernels: 102 us -> 104 us
  other arithmetic: 1.46 us -> 0 us
    pallas_call x1, Pallas kernels: 102 us -> 104 us  [local(): pl.pallas_call(functools.partial(layer_kernel, names, head_width, PIECES,...]
    reduce_sum x1 -> x0, other arithmetic: 1.46 us -> none  [shares_of(): jnp.sum(jnp.where(routed_expert_index[:, :, None] == ids, routed_expert_w...]
where the time goes in v3:
time: 106 us
  Pallas kernels  104 us (98%)
  local copies, waits for them, and re-layouts  1.88 us (2%)
    pallas_call x1, Pallas kernels, local(): pl.pallas_call(functools.partial(layer_kernel, names, head_width, PIECES,...  104 us

profile of v3, /device:TPU:0, one launch (start us, length us, event | category | flops | bytes accessed | tf_op | source)
XLA Modules:
  0.0 106.2 jit_solution(8071335005362010974)
XLA Ops:
  0.0 104.3 %layer.1 = bf16[128,2048]{1,0:T(8,128)(2,1)} custom-call(bf16[512,512]{1,0:T(8,128)(2,1)} %all_refs_0_.1, bf16[512,512]{1,0:T(8,128)(2,1)} %all_refs_1_.1, bf16[512,512]{1,0:T(8,128)(2,1)} %all_refs_2_.1, bf16[512,512]{1,0:T(8,128)(2,1)} %all_refs_3_.1, bf16[512,512]{1,0:T(8,128)(2,1)} %all_refs_4_.1, f32[8,512]{1,0:T(8,128)} %bitcast.14, ...), custom_call_target="tpu_custom_call" | custom-call | flops 30000001024 | bytes 10485760 | tf_op jit(solution)/shard_map/layer/pallas_call | solution.py:950
  104.3 1.9 %copy.21 = bf16[128,2048]{1,0:T(8,128)(2,1)} copy(bf16[128,2048]{1,0:T(8,128)(2,1)} %layer.1) | data formatting | bytes 1048576
